TPU v7x, 32 devices: a whole 2x2x4 slice. The times are simulated.
32 devices in a mesh: ep: 8 (over z, x), tp: 4 (over y, core).
Axes of the slice: x: 2, y: 2, z: 4, core: 2. Of those that a mesh axis runs over, the one named last changes fastest.
Arguments:
- tokens: bfloat16 [64, 2048], P('ep'), may hold values from -6 to 6
- mix_gain: bfloat16 [2048], replicated, may hold values from 0.099609375 to 1.8984375
- w_query: bfloat16 [2048, 512], P(None, 'tp'), may hold values from -0.125 to 0.125
- w_key: bfloat16 [2048, 512], P(None, 'tp'), may hold values from -0.125 to 0.125
- w_value: bfloat16 [2048, 512], P(None, 'tp'), may hold values from -0.125 to 0.125
- w_igate: bfloat16 [2048, 4], replicated, may hold values from -0.125 to 0.125
- w_fgate: bfloat16 [2048, 4], replicated, may hold values from -0.125 to 0.125
- forget_bias: float32 [4], replicated, may hold values from 0.5 to 4.5
- w_out: bfloat16 [512, 2048], P('tp'), may hold values from -0.25 to 0.25
- mem_state: float32 [64, 4, 16384], P('ep', 'tp'), may hold values from -0.75 to 0.75
- norm_state: float32 [64, 512], P('ep', 'tp'), may hold values from -0.75 to 0.75
- max_state: float32 [64, 4], P('ep', 'tp'), may hold values from -3 to 3
- ffn_gain: bfloat16 [2048], replicated, may hold values from 0.099609375 to 1.8984375
- route_ids: int32 [64, 2], P('ep'), may hold values from 0 to 7, all different within a row; in each aligned block of 8 rows (0 to 7, 8 to 15, ...) at most 3 rows name the same one
- route_weights: float32 [64, 2], P('ep'), may hold values from 0.1 to 1
- w_gate: bfloat16 [2048, 32768], P(None, ('ep', 'tp')), may hold values from -0.125 to 0.125
- w_up: bfloat16 [2048, 32768], P(None, ('ep', 'tp')), may hold values from -0.125 to 0.125
- w_down: bfloat16 [32768, 2048], P('ep', 'tp'), may hold values from -0.09375 to 0.09375
Outputs:
- out_tokens: bfloat16 [64, 2048], P('ep', 'tp')
- new_memory: float32 [64, 4, 16384], P('ep', 'tp')
- new_norm: float32 [64, 512], P('ep', 'tp')
- new_max: float32 [64, 4], P('ep', 'tp')
Inputs may be any that keep to these rules, and one draw needn't show every extreme that they name: `route_ids`: each row names 2 different experts; among the rows of one index of ep no expert is named more than 3 times, a bound that some block reaches.
All inputs are finite; a program needn't handle non-finite values.
Results may differ from a plain program's by a relative error of at most 0.013.
The roundings to bfloat16 on the way count: a program that leaves them out, or rounds other values in their place, can miss the bound.
Values may be sent and summed in bfloat16 or wider, within the bound.
No kernel may reach another device: no remote copies, remote signals or barrier semaphores. Data moves between devices by JAX's collectives and lax.ppermute only.
A program may use at most 64 MiB of HBM per device.

v0:
```python
import functools
import jax
import jax.numpy as jnp
from jax import lax
from jax.experimental import pallas as pl
from jax.experimental.pallas import tpu as pltpu
from jax.sharding import PartitionSpec as P

FF = 4096
LANES = 128
epsilon = 1e-06
f32 = jnp.float32
bf16 = jnp.bfloat16


VMEM = pl.BlockSpec(memory_space=pltpu.VMEM)
ANY = pl.BlockSpec(memory_space=pl.ANY)


def kernel_call(body, outs, ins, in_specs=None, out_specs=None, scratch=(), cost=1000, limit=None):
    return pl.pallas_call(
        body,
        out_shape=outs,
        in_specs=in_specs or [VMEM] * len(ins),
        out_specs=out_specs or tuple([VMEM] * len(outs)),
        scratch_shapes=list(scratch),
        compiler_params=pltpu.CompilerParams(vmem_limit_bytes=limit),
        cost_estimate=pl.CostEstimate(flops=cost, bytes_accessed=0, transcendentals=0),
    )(*ins)


def scaled_tiles(wide, gain_ref):
    width = wide.shape[1]
    factor = lax.rsqrt(jnp.sum(wide * wide, 1, keepdims=True) / width + epsilon)
    gain = gain_ref[...].astype(f32)
    tiles = [
        wide[:, at * LANES : (at + 1) * LANES] * factor * gain[at : at + 1, :]
        for at in range(width // LANES)
    ]
    return jnp.concatenate(tiles, 1).astype(bf16)


def to_column(row):
    count = row.shape[1]
    eye = lax.broadcasted_iota(jnp.int32, (count, count), 0) == lax.broadcasted_iota(
        jnp.int32, (count, count), 1
    )
    return jnp.sum(jnp.where(eye, jnp.broadcast_to(row, (count, count)), 0.0), 1, keepdims=True)


def to_row(column):
    count = column.shape[0]
    eye = lax.broadcasted_iota(jnp.int32, (count, count), 0) == lax.broadcasted_iota(
        jnp.int32, (count, count), 1
    )
    return jnp.sum(jnp.where(eye, jnp.broadcast_to(column, (count, count)), 0.0), 0, keepdims=True)


def routing(ids, weights, rows, slots, spans, base, paired=0):
    top_count, seq_count = ids.shape
    at = lax.broadcasted_iota(jnp.int32, (rows, seq_count), 0)
    if paired:
        slot = (at // paired % slots).astype(f32)
        block = at % paired * 2 + at // (paired * slots)
    else:
        slot = (at % slots).astype(f32)
        block = at // slots
    expert = (block ^ base) // spans
    named = jnp.zeros((rows, seq_count), f32)
    weighted = jnp.zeros((rows, seq_count), f32)
    for k in range(top_count):
        hit = expert == ids[k : k + 1, :]
        named = named + jnp.where(hit, 1.0, 0.0)
        weighted = weighted + jnp.where(hit, weights[k : k + 1, :], 0.0)
    before = jnp.where(
        lax.broadcasted_iota(jnp.int32, (seq_count, seq_count), 0)
        < lax.broadcasted_iota(jnp.int32, (seq_count, seq_count), 1),
        1.0,
        0.0,
    )
    rank = jnp.dot(named, before, preferred_element_type=f32)
    mine = rank == slot
    return jnp.where(mine, named, 0.0), jnp.where(mine, weighted, 0.0)


def cell_kernel(
    slots, spans, paired,
    tokens_hbm, gain_hbm, next_gain_hbm, wq_hbm, wk_hbm, wv_hbm, wi_hbm, wf_hbm, bias_hbm, mem_hbm, norm_hbm,
    max_hbm, wo_hbm, ids_hbm, weights_hbm,
    partial_ref, keys_ref, values_ref, keep_ref, norm_out, max_out, placing_ref, mixing_ref, tokens_ref,
    next_gain_ref,
    gain_ref, wq_ref, wk_ref, wv_ref, wi_ref, wf_ref, bias_ref, mem_ref, norm_ref, max_ref, wo_ref, ids_ref,
    weights_ref, sems,
):
    pairs = (
        (tokens_hbm, tokens_ref), (gain_hbm, gain_ref), (ids_hbm, ids_ref), (weights_hbm, weights_ref),
        (wi_hbm, wi_ref), (wf_hbm, wf_ref), (bias_hbm, bias_ref), (max_hbm, max_ref), (norm_hbm, norm_ref),
        (wk_hbm, wk_ref), (wq_hbm, wq_ref), (mem_hbm, mem_ref), (wv_hbm, wv_ref), (wo_hbm, wo_ref),
        (next_gain_hbm, next_gain_ref),
    )
    copies = [pltpu.make_async_copy(a, b, sems.at[i]) for i, (a, b) in enumerate(pairs)]
    for copy in copies:
        copy.start()

    def arrive(first, last):
        for copy in copies[first:last]:
            copy.wait()

    head = lax.axis_index("tp")
    seq_count = tokens_ref.shape[0]
    head_dim = wq_ref.shape[1]
    arrive(0, 2)
    normed = scaled_tiles(tokens_ref[...].astype(f32), gain_ref)

    def project(ref):
        return jnp.dot(normed, ref[...], preferred_element_type=f32).astype(bf16).astype(f32)

    def gate(ref):
        return lax.dot_general(
            normed, ref[...], (((1,), (1,)), ((), ())), preferred_element_type=f32
        )

    arrive(2, 9)
    base = lax.axis_index("ep") if paired else 0
    shape = ids_ref[...], weights_ref[...], mixing_ref.shape[0], slots, spans, base
    placing, mixing = routing(*shape)
    if paired:
        placing, _ = routing(*shape, paired)
    placing_ref[...] = placing.astype(bf16)
    mixing_ref[...] = mixing
    inputs = gate(wi_ref)
    forgets = gate(wf_ref) + bias_ref[...]
    here = lax.broadcasted_iota(jnp.int32, inputs.shape, 1) == head
    input_gate = jnp.sum(jnp.where(here, inputs, 0.0), 1, keepdims=True)
    forget = jnp.sum(jnp.where(here, forgets, 0.0), 1, keepdims=True)
    forget_log = jnp.minimum(forget, 0.0) - jnp.log1p(jnp.exp(-jnp.abs(forget)))
    held = forget_log + to_column(max_ref[...])
    new_max = jnp.maximum(held, input_gate)
    keep = jnp.exp(held - new_max)
    fresh = jnp.exp(input_gate - new_max)
    max_out[...] = to_row(new_max)
    keep_ref[...] = jnp.broadcast_to(keep, keep_ref.shape)
    arrive(9, 10)
    key = project(wk_ref) * head_dim ** (-0.5)
    arrive(10, 11)
    query = project(wq_ref)
    query_t = query.T
    match = jnp.sum(query * key, 1, keepdims=True)
    new_norm = keep * norm_ref[...] + fresh * key
    norm_out[...] = new_norm
    keys_ref[...] = fresh * key
    denominator = jnp.sum(query * new_norm, 1, keepdims=True)
    scale = jnp.maximum(jnp.abs(denominator), jnp.exp(-new_max))
    arrive(11, 12)
    read = []
    for s in range(seq_count):
        read.append(jnp.sum(mem_ref[s] * query_t[:, s : s + 1], 0, keepdims=True))
    read = jnp.concatenate(read, 0)
    arrive(12, 13)
    value = project(wv_ref)
    values_ref[...] = value
    readout = (keep * read + (fresh * match) * value) / scale
    arrive(13, 14)
    partial_ref[...] = jnp.dot(
        readout.astype(bf16), wo_ref[...], preferred_element_type=f32
    ).astype(bf16)
    arrive(14, 15)


def pack_kernel(groups, tick_ref, tokens_ref, gain_ref, placing_ref, *refs):
    partials, outs, residual_ref = refs[: -groups - 1], refs[-groups - 1 : -1], refs[-1]
    total = partials[0][...].astype(f32)
    for ref in partials[1:]:
        total = total + ref[...].astype(f32)
    residual = (tokens_ref[...].astype(f32) + total).astype(bf16)
    residual_ref[...] = residual
    normed = scaled_tiles(residual.astype(f32), gain_ref)
    rows = jnp.dot(placing_ref[...], normed, preferred_element_type=f32).astype(bf16)
    if groups == 1:
        spread(rows, outs[0])
        return
    count, width = outs[0].shape[0], rows.shape[1]
    slots = outs[0].shape[1] // width
    for g, out_ref in enumerate(outs):
        for c in range(slots):
            start = (g * slots + c) * count
            out_ref[:, c * width : (c + 1) * width] = rows[start : start + count, :]


def spread(rows, out_ref):
    slots = out_ref.shape[1]
    for at in range(out_ref.shape[0]):
        out_ref[at] = rows[at * slots : (at + 1) * slots, :].astype(bf16)


def join_kernel(near_ref, far_ref, *outs):
    for at, out_ref in enumerate(outs):
        out_ref[0] = near_ref[at]
        out_ref[1] = far_ref[at]


def split_join_kernel(tick_ref, near_ref, far_ref, own_ref, first_ref, second_ref):
    near, far = near_ref[...].astype(f32), far_ref[...].astype(f32)

    def pair(at):
        return jnp.concatenate([near[at : at + 1, :], far[at : at + 1, :]], 0)

    odd = lax.axis_index("tp") & 1 == 1
    own_ref[...] = pair(0).astype(bf16)
    first_ref[...] = jnp.where(odd, pair(3), pair(1)).astype(bf16)
    second_ref[...] = pair(2).astype(bf16)


def fetch_kernel(tick_ref, source_ref, target_ref, sems):
    pieces = sems.shape[0]
    height = source_ref.shape[0] // pieces
    copies = []
    for at in range(pieces):
        rows = pl.ds(at * height, height)
        copies.append(
            pltpu.make_async_copy(source_ref.at[rows], target_ref.at[rows], sems.at[at])
        )
    for copy in copies:
        copy.start()
    for copy in copies:
        copy.wait()


def fetched(weight, after):
    return kernel_call(
        fetch_kernel,
        (pltpu.VMEM(weight.shape, weight.dtype),),
        (after, *in_hbm(weight)),
        in_specs=[ANY] * 2,
        out_specs=(ANY,),
        scratch=[pltpu.SemaphoreType.DMA((8,))],
        cost=20_000_000,
        limit=1 << 20,
    )[0]


def stacked(refs):
    return jnp.concatenate(
        [ref[at].astype(f32) for ref in refs for at in range(ref.shape[0])], 0
    )


def expert_kernel(*refs):
    *parts, gate_ref, up_ref, out_ref = refs
    deep = gate_ref.shape[0]
    if len(parts) == 1:
        rows = stacked(parts).astype(bf16)
    else:
        own, first, second, other_first, other_second = [ref[...].astype(f32) for ref in parts]
        odd = lax.axis_index("tp") & 1 == 1
        pieces = []
        for part in (
            own,
            jnp.where(odd, other_first, first),
            jnp.where(odd, second, other_second),
            jnp.where(odd, first, other_first),
        ):
            pieces += [part[:, at : at + deep] for at in range(0, part.shape[1], deep)]
        rows = jnp.concatenate(pieces, 0).astype(bf16)
    width = out_ref.shape[1]
    step = min(width, 512)
    for at in range(0, width, step):
        gate_sum = jnp.dot(rows, gate_ref[:, at : at + step], preferred_element_type=f32)
        up_sum = jnp.dot(rows, up_ref[:, at : at + step], preferred_element_type=f32)
        out_ref[:, at : at + step] = (gate_sum * jax.nn.sigmoid(gate_sum) * up_sum).astype(bf16)


def down_term(hidden_ref, weight_ref, k):
    units = hidden_ref.shape[1]
    start = pl.multiple_of((lax.axis_index("tp") ^ k) * units, units)
    return jnp.dot(
        hidden_ref[...], weight_ref[pl.ds(start, units), :], preferred_element_type=f32
    )


def first_down_kernel(near_ref, weight_ref, total_ref):
    total_ref[...] = down_term(near_ref, weight_ref, 0)


def down_kernel(tp_count, total_ref, *refs):
    hiddens, weight_ref, outs = refs[: tp_count - 1], refs[tp_count - 1], refs[tp_count:]
    total = total_ref[...]
    for k, hidden_ref in enumerate(hiddens):
        total = total + down_term(hidden_ref, weight_ref, 1 + k)
    if len(outs) == 1:
        spread(total, outs[0])
        return
    slots, count = outs[0].shape[1], len(outs)
    for g, out_ref in enumerate(outs):
        for at in range(out_ref.shape[0]):
            picked = [(at * slots + c) * count + g for c in range(slots)]
            out_ref[at] = jnp.concatenate([total[r : r + 1, :] for r in picked], 0).astype(bf16)


def state_kernel(tick_ref, mem_ref, keys_ref, values_ref, keep_ref, norm_ref, max_ref, out_ref, norm_out, max_out):
    norm_out[...] = norm_ref[...]
    max_out[...] = max_ref[...]
    keys_t = keys_ref[...].T
    value = values_ref[...]
    for s in range(mem_ref.shape[0]):
        out_ref[s] = (
            keep_ref[s : s + 1, :] * mem_ref[s] + keys_t[:, s : s + 1] * value[s : s + 1, :]
        )


def final_kernel(residual_ref, mixing_ref, *refs):
    *parts, out_ref = refs
    width = out_ref.shape[1]
    start = pl.multiple_of(lax.axis_index("tp") * width, width)
    routed = lax.dot_general(
        mixing_ref[...],
        stacked(parts),
        (((0,), (0,)), ((), ())),
        precision=lax.Precision.HIGHEST,
        preferred_element_type=f32,
    )
    out_ref[...] = (residual_ref[:, pl.ds(start, width)].astype(f32) + routed).astype(bf16)


def in_hbm(*values):
    return [pltpu.with_memory_space_constraint(value, pltpu.HBM) for value in values]


def swapped(value, axis, bits):
    count = lax.axis_size(axis)
    return lax.ppermute(value, axis, [(at, at ^ bits) for at in range(count)])


def sent(value, target):
    ep_count, tp_count = lax.axis_size("ep"), lax.axis_size("tp")
    pairs = []
    for e in range(ep_count):
        for t in range(tp_count):
            to_e, to_t = target(e, t)
            pairs.append((e * tp_count + t, to_e * tp_count + to_t))
    return lax.ppermute(value, ("ep", "tp"), pairs)


def from_partners(value, count):
    moved = [swapped(value, "tp", k) for k in reversed(range(1, count))]
    return [value, *reversed(moved)]


def gathered(near, far, w_up):
    came = swapped(far, "ep", 1)
    up_w = fetched(w_up, far)
    pair = (2, near.shape[1])
    own, first, second = kernel_call(
        split_join_kernel,
        tuple(pltpu.VMEM(pair, near.dtype) for _ in range(3)),
        (up_w, near, came),
        in_specs=[ANY, VMEM, VMEM],
        limit=4 << 20,
    )
    first = sent(first, lambda e, t: (e ^ 6, t) if t & 1 else (e ^ 2, t))
    second = sent(second, lambda e, t: (e ^ 4, t) if t & 1 else (e, t ^ 2))
    shared = [swapped(part, "tp", 1) for part in (first, second)]
    return [own, first, second, *shared], up_w


def returned_blocks(near, far):
    came = swapped(far, "ep", 1)
    count, *block = near.shape
    joined = kernel_call(
        join_kernel,
        tuple(pltpu.VMEM((2, *block), near.dtype) for _ in range(count)),
        (near, came),
        limit=4 << 20,
    )
    moved = [swapped(joined[k], "ep", 2 * k) for k in reversed(range(1, count))]
    return [joined[0], *reversed(moved)], joined[1]


def shards(
    tokens, mix_gain, w_query, w_key, w_value, w_igate, w_fgate, forget_bias, w_out, mem_state, norm_state,
    max_state, ffn_gain, route_ids, route_weights, w_gate, w_up, w_down,
):
    seq_count, model_width = tokens.shape
    head_dim = norm_state.shape[1]
    tp_count = lax.axis_size("tp")
    ep_count = lax.axis_size("ep")
    own_width = model_width // tp_count
    top_count = route_ids.shape[1]
    spans = FF // w_down.shape[0]
    experts = ep_count // spans
    bound = max(2, 3 * seq_count * top_count // (2 * experts))
    slots = bound
    rows = ep_count * slots
    struct = jax.ShapeDtypeStruct
    direct = ep_count <= 8
    groups = 2 if direct else 1

    def block_outs(width):
        if direct:
            return tuple(pltpu.VMEM((ep_count // 2, slots, width), bf16) for _ in range(2))
        return (struct((ep_count, slots, width), bf16),)

    memory = mem_state.reshape(seq_count, head_dim, head_dim)
    gain_shape = (model_width // LANES, LANES)
    sources = (
        tokens, mix_gain.reshape(gain_shape), ffn_gain.reshape(gain_shape), w_query, w_key, w_value, w_igate.T,
        w_fgate.T, forget_bias.reshape(1, -1), memory, norm_state, max_state.T, w_out, route_ids.T,
        route_weights.T,
    )
    partial, keys, values, keep, new_norm, new_max, placing, mixing, rows_in, gain_b = kernel_call(
        functools.partial(cell_kernel, slots, spans, ep_count // 2 if direct else 0),
        (
            pltpu.VMEM((seq_count, model_width), bf16),
            pltpu.VMEM((seq_count, head_dim), f32),
            pltpu.VMEM((seq_count, head_dim), f32),
            pltpu.VMEM((seq_count, head_dim), f32),
            pltpu.VMEM((seq_count, head_dim), f32),
            pltpu.VMEM((1, seq_count), f32),
            pltpu.VMEM((rows, seq_count), bf16),
            pltpu.VMEM((rows, seq_count), f32),
            pltpu.VMEM((seq_count, model_width), bf16),
            pltpu.VMEM(gain_shape, bf16),
        ),
        in_hbm(*sources),
        in_specs=[ANY] * len(sources),
        scratch=[
            *(pltpu.VMEM(v.shape, v.dtype) for v in (sources[1], *sources[3:])),
            pltpu.SemaphoreType.DMA((len(sources),)),
        ],
        limit=16 << 20,
    )
    partials = from_partners(partial, tp_count)
    gate_w = fetched(w_gate, partial)
    if direct:
        packed_outs = [pltpu.VMEM((ep_count // 2, slots * model_width), bf16) for _ in range(2)]
    else:
        packed_outs = block_outs(model_width)
    *blocks, residual = kernel_call(
        functools.partial(pack_kernel, groups),
        (*packed_outs, pltpu.VMEM((seq_count, model_width), bf16)),
        (gate_w, rows_in, gain_b, placing, *partials),
        in_specs=[ANY] + [VMEM] * (3 + tp_count),
        limit=16 << 20,
    )
    if direct:
        arrived, up_w = gathered(*blocks, w_up)
    else:
        arrived = [lax.all_to_all(blocks[0], "ep", split_axis=0, concat_axis=0, tiled=True)]
        up_w = fetched(w_up, blocks[0])
    (hidden,) = kernel_call(
        expert_kernel,
        (pltpu.VMEM((rows, w_gate.shape[1]), bf16),),
        (*arrived, gate_w, up_w),
        limit=8 << 20,
    )
    hiddens = from_partners(hidden, tp_count)
    down_w = fetched(w_down, hidden)
    (total,) = kernel_call(
        first_down_kernel,
        (pltpu.VMEM((rows, own_width), f32),),
        (hidden, down_w),
        cost=2_000_000,
        limit=8 << 20,
    )
    blocks = kernel_call(
        functools.partial(down_kernel, tp_count),
        block_outs(own_width),
        (total, *hiddens[1:], down_w),
        limit=8 << 20,
    )

    def state(tick):
        return kernel_call(
            state_kernel,
            (
                struct((seq_count, head_dim, head_dim), f32),
                struct((seq_count, head_dim), f32),
                struct((1, seq_count), f32),
            ),
            (tick, memory, keys, values, keep, new_norm, new_max),
            in_specs=[ANY] + [VMEM] * 6,
            cost=20_000_000,
            limit=8 << 20,
        )

    if direct:
        returned, tick = returned_blocks(*blocks)
    else:
        tick = blocks[0]
        returned = [lax.all_to_all(tick, "ep", split_axis=0, concat_axis=0, tiled=True)]
    new_memory, new_norm, new_max = state(tick)
    (out_tokens,) = kernel_call(
        final_kernel,
        (struct((seq_count, own_width), bf16),),
        (residual, mixing, *returned),
        limit=8 << 20,
    )
    return (
        out_tokens,
        new_memory.reshape(mem_state.shape),
        new_norm,
        new_max.T,
    )


def solution(mesh):
    placed = (
        P("ep", None),
        P(),
        P(None, "tp"),
        P(None, "tp"),
        P(None, "tp"),
        P(),
        P(),
        P(),
        P("tp", None),
        P("ep", "tp", None),
        P("ep", "tp"),
        P("ep", "tp"),
        P(),
        P("ep", None),
        P("ep", None),
        P(None, ("ep", "tp")),
        P(None, ("ep", "tp")),
        P("ep", "tp"),
    )

    return jax.shard_map(
        shards,
        mesh=mesh,
        in_specs=placed,
        out_specs=(P("ep", "tp"), P("ep", "tp", None), P("ep", "tp"), P("ep", "tp")),
        check_vma=False,
    )
```

profile of v0, /device:TPU:0, one launch (start us, length us, event | category | flops | bytes accessed | tf_op | source)
XLA Modules:
  0.0 40.8 jit_solution(9909197833478167757)
XLA Ops:
  0.6 2.4 %shard_map.201 = (bf16[8,2048]{1,0:T(8,128)(2,1)S(1)}, f32[8,128]{1,0:T(8,128)S(1)}, f32[8,128]{1,0:T(8,128)S(1)}, f32[8,128]{1,0:T(8,128)S(1)}, f32[8,128]{1,0:...) custom-call(bf16[8,2048]{1,0:T(8,128)(2,1)} %tokens_hbm.1, ...), custom_call_target="tpu_custom_call" | custom-call | flops 1000 | tf_op jit(solution)/shard_map/pallas_call | solution.py:21
  3.0 2.5 %collective-permute-start.2 = (bf16[8,2048]{1,0:T(8,128)(2,1)S(1)}, bf16[8,2048]{1,0:T(8,128)(2,1)S(1)}, u32[]{:S(2)}, u32[]{:S(2)}) collective-permute-start(bf16[8,2048]{1,0:T(8,128)(2,1)S(1)} %get-tuple-element.29.tick_ref.refs_0_), channel_id=1, source_target_pairs={{0,3},{1,2},{2,1},{3,0},{4,7},{5,6},{6,5},{7,4},{8,11},{9,10},{10,... | collective-permute-start | bytes 98312 | tf_op jit(solution)/shard_map/ppermute | solution.py:331
  6.2 2.2 %shard_map.202.tick_ref.refs_5_ = bf16[2048,1024]{1,0:T(8,128)(2,1)S(1)} custom-call(bf16[8,2048]{1,0:T(8,128)(2,1)S(1)} %get-tuple-element.29.tick_ref.refs_0_, bf16[2048,1024]{1,0:T(8,128)(2,1)} %source_ref.3), custom_call_target="tpu_custom_call" | custom-call | flops 20000000 | tf_op jit(solution)/shard_map/pallas_call | solution.py:21
  8.5 1.1 %collective-permute-done.1.refs_2_ = bf16[8,2048]{1,0:T(8,128)(2,1)S(1)} collective-permute-done((bf16[8,2048]{1,0:T(8,128)(2,1)S(1)}, bf16[8,2048]{1,0:T(8,128)(2,1)S(1)}, u32[]{:S(2)}, u32[]{:S(2)}) %collective-permute-start.1) | collective-permute-done | bytes 32800 | tf_op jit(solution)/shard_map/ppermute | solution.py:331
  9.8 1.6 %collective-permute-start.3 = (bf16[4,6144]{1,0:T(4,128)(2,1)S(1)}, bf16[4,6144]{1,0:T(4,128)(2,1)S(1)}, u32[]{:S(2)}, u32[]{:S(2)}) collective-permute-start(bf16[4,6144]{1,0:T(4,128)(2,1)S(1)} %get-tuple-element.35.tick_ref), channel_id=1, source_target_pairs={{0,4},{4,0},{8,12},{12,8},{16,20},{20,16},{24,28},{28,24},{1,5},{5... | collective-permute-start | bytes 147464 | tf_op jit(solution)/shard_map/ppermute | solution.py:331
  11.4 2.2 %shard_map.204.tick_ref.refs_6_ = bf16[2048,1024]{1,0:T(8,128)(2,1)S(1)} custom-call(bf16[4,6144]{1,0:T(4,128)(2,1)S(1)} %get-tuple-element.35.tick_ref, bf16[2048,1024]{1,0:T(8,128)(2,1)} %source_ref.4), custom_call_target="tpu_custom_call" | custom-call | flops 20000000 | tf_op jit(solution)/shard_map/pallas_call | solution.py:21
  14.1 1.6 %collective-permute-start.4 = (bf16[2,6144]{1,0:T(2,128)(2,1)S(1)}, bf16[2,6144]{1,0:T(2,128)(2,1)S(1)}, u32[]{:S(2)}, u32[]{:S(2)}) collective-permute-start(bf16[2,6144]{1,0:T(2,128)(2,1)S(1)} %get-tuple-element.38), channel_id=1, source_target_pairs={{0,8},{1,25},{2,10},{3,27},{4,12},{5,29},{6,14},{7,31},{8,0},{9,17... | collective-permute-start | bytes 73736 | tf_op jit(solution)/shard_map/ppermute | solution.py:341
  15.7 1.0 %collective-permute-start.5 = (bf16[2,6144]{1,0:T(2,128)(2,1)S(1)}, bf16[2,6144]{1,0:T(2,128)(2,1)S(1)}, u32[]{:S(2)}, u32[]{:S(2)}) collective-permute-start(bf16[2,6144]{1,0:T(2,128)(2,1)S(1)} %get-tuple-element.39), channel_id=1, source_target_pairs={{0,2},{1,17},{2,0},{3,19},{4,6},{5,21},{6,4},{7,23},{8,10},{9,25},... | collective-permute-start | bytes 73736 | tf_op jit(solution)/shard_map/ppermute | solution.py:341
  16.7 1.5 %collective-permute-done.4.refs_1_ = bf16[2,6144]{1,0:T(2,128)(2,1)S(1)} collective-permute-done((bf16[2,6144]{1,0:T(2,128)(2,1)S(1)}, bf16[2,6144]{1,0:T(2,128)(2,1)S(1)}, u32[]{:S(2)}, u32[]{:S(2)}) %collective-permute-start.4) | collective-permute-done | bytes 24608 | tf_op jit(solution)/shard_map/ppermute | solution.py:341
  18.2 1.3 %collective-permute-done.5.refs_2_ = bf16[2,6144]{1,0:T(2,128)(2,1)S(1)} collective-permute-done((bf16[2,6144]{1,0:T(2,128)(2,1)S(1)}, bf16[2,6144]{1,0:T(2,128)(2,1)S(1)}, u32[]{:S(2)}, u32[]{:S(2)}) %collective-permute-start.5) | collective-permute-done | bytes 24608 | tf_op jit(solution)/shard_map/ppermute | solution.py:341
  19.6 0.7 %collective-permute-start.7 = (bf16[2,6144]{1,0:T(2,128)(2,1)S(1)}, bf16[2,6144]{1,0:T(2,128)(2,1)S(1)}, u32[]{:S(2)}, u32[]{:S(2)}) collective-permute-start(bf16[2,6144]{1,0:T(2,128)(2,1)S(1)} %collective-permute-done.5.refs_2_), channel_id=1, source_target_pairs={{0,1},{1,0},{2,3},{3,2},{4,5},{5,4},{6,7},{7,6},{8,9},{9,8},{10,11... | collective-permute-start | bytes 73736 | tf_op jit(solution)/shard_map/ppermute | solution.py:331
  20.2 0.8 %collective-permute-done.7.refs_4_ = bf16[2,6144]{1,0:T(2,128)(2,1)S(1)} collective-permute-done((bf16[2,6144]{1,0:T(2,128)(2,1)S(1)}, bf16[2,6144]{1,0:T(2,128)(2,1)S(1)}, u32[]{:S(2)}, u32[]{:S(2)}) %collective-permute-start.7) | collective-permute-done | bytes 24608 | tf_op jit(solution)/shard_map/ppermute | solution.py:331
  21.1 1.6 %shard_map.206.tick_ref.near_ref = bf16[24,1024]{1,0:T(8,128)(2,1)S(1)} custom-call(bf16[2,6144]{1,0:T(2,128)(2,1)S(1)} %get-tuple-element.37.refs_0_, bf16[2,6144]{1,0:T(2,128)(2,1)S(1)} %collective-permute-done.4.refs_1_, bf16[2,6144]{1,0:T(2,128)(2,1)S(1)} %collective-permute-done.5.refs_2_, bf16[2,6144]{1,0:T(2,128)(2,1)S(1)} %collective-permute-done.6.refs_3_, ...), custom_call_target="tpu_custom_call" | custom-call | flops 1000 | tf_op jit(solution)/shard_map/pallas_call | solution.py:21
  22.6 1.2 %collective-permute-start.10 = (bf16[24,1024]{1,0:T(8,128)(2,1)S(1)}, bf16[24,1024]{1,0:T(8,128)(2,1)S(1)}, u32[]{:S(2)}, u32[]{:S(2)}) collective-permute-start(bf16[24,1024]{1,0:T(8,128)(2,1)S(1)} %shard_map.206.tick_ref.near_ref), channel_id=1, source_target_pairs={{0,3},{1,2},{2,1},{3,0},{4,7},{5,6},{6,5},{7,4},{8,11},{9,10},{10,... | collective-permute-start | bytes 147464 | tf_op jit(solution)/shard_map/ppermute | solution.py:331
  23.9 0.8 %collective-permute-start.9 = (bf16[24,1024]{1,0:T(8,128)(2,1)S(1)}, bf16[24,1024]{1,0:T(8,128)(2,1)S(1)}, u32[]{:S(2)}, u32[]{:S(2)}) collective-permute-start(bf16[24,1024]{1,0:T(8,128)(2,1)S(1)} %shard_map.206.tick_ref.near_ref), channel_id=1, source_target_pairs={{0,2},{1,3},{2,0},{3,1},{4,6},{5,7},{6,4},{7,5},{8,10},{9,11},{10,... | collective-permute-start | bytes 147464 | tf_op jit(solution)/shard_map/ppermute | solution.py:331
  24.6 2.2 %shard_map.207.weight_ref.refs_3_ = bf16[4096,512]{1,0:T(8,128)(2,1)S(1)} custom-call(bf16[24,1024]{1,0:T(8,128)(2,1)S(1)} %shard_map.206.tick_ref.near_ref, bf16[4096,512]{1,0:T(8,128)(2,1)} %source_ref.5), custom_call_target="tpu_custom_call" | custom-call | flops 20000000 | tf_op jit(solution)/shard_map/pallas_call | solution.py:21
  27.2 0.8 %collective-permute-done.9.refs_1_ = bf16[24,1024]{1,0:T(8,128)(2,1)S(1)} collective-permute-done((bf16[24,1024]{1,0:T(8,128)(2,1)S(1)}, bf16[24,1024]{1,0:T(8,128)(2,1)S(1)}, u32[]{:S(2)}, u32[]{:S(2)}) %collective-permute-start.9) | collective-permute-done | bytes 49184 | tf_op jit(solution)/shard_map/ppermute | solution.py:331
  28.6 1.0 %collective-permute-start.11 = (bf16[4,3,512]{2,1,0:T(4,128)(2,1)S(1)}, bf16[4,3,512]{2,1,0:T(4,128)(2,1)S(1)}, u32[]{:S(2)}, u32[]{:S(2)}) collective-permute-start(bf16[4,3,512]{2,1,0:T(4,128)(2,1)S(1)} %get-tuple-element.41), channel_id=1, source_target_pairs={{0,4},{4,0},{8,12},{12,8},{16,20},{20,16},{24,28},{28,24},{1,5},{5... | collective-permute-start | bytes 36872 | tf_op jit(solution)/shard_map/ppermute | solution.py:331
  29.7 2.8 %collective-permute-done.11.far_ref = bf16[4,3,512]{2,1,0:T(4,128)(2,1)S(1)} collective-permute-done((bf16[4,3,512]{2,1,0:T(4,128)(2,1)S(1)}, bf16[4,3,512]{2,1,0:T(4,128)(2,1)S(1)}, u32[]{:S(2)}, u32[]{:S(2)}) %collective-permute-start.11) | collective-permute-done | bytes 12320 | tf_op jit(solution)/shard_map/ppermute | solution.py:331
  32.4 2.1 %collective-permute-start.13 = (bf16[2,3,512]{2,1,0:T(4,128)(2,1)S(1)}, bf16[2,3,512]{2,1,0:T(4,128)(2,1)S(1)}, u32[]{:S(2)}, u32[]{:S(2)}) collective-permute-start(bf16[2,3,512]{2,1,0:T(4,128)(2,1)S(1)} %get-tuple-element.44), channel_id=1, source_target_pairs={{0,16},{4,20},{8,24},{12,28},{16,0},{20,4},{24,8},{28,12},{1,17},{... | collective-permute-start | bytes 18440 | tf_op jit(solution)/shard_map/ppermute | solution.py:331
  34.8 1.2 %collective-permute-start.12 = (bf16[2,3,512]{2,1,0:T(4,128)(2,1)S(1)}, bf16[2,3,512]{2,1,0:T(4,128)(2,1)S(1)}, u32[]{:S(2)}, u32[]{:S(2)}) collective-permute-start(bf16[2,3,512]{2,1,0:T(4,128)(2,1)S(1)} %get-tuple-element.43.tick_ref), channel_id=1, source_target_pairs={{0,8},{4,12},{8,0},{12,4},{16,24},{20,28},{24,16},{28,20},{1,9},{5... | collective-permute-start | bytes 18440 | tf_op jit(solution)/shard_map/ppermute | solution.py:331
  36.0 1.1 %shard_map.212 = (f32[8,128,128]{2,1,0:T(8,128)}, f32[8,128]{1,0:T(8,128)}, f32[1,8]{1,0:T(1,128)}) custom-call(bf16[2,3,512]{2,1,0:T(4,128)(2,1)S(1)} %get-tuple-element.43.tick_ref, f32[8,128,128]{2,1,0:T(8,128)S(1)} %bitcast.12, f32[8,128]{1,0:T(8,128)S(1)} %get-tuple-element.46.keys_ref, f32[8,128]{1,0:T(8,128)S(1)} %get-tuple-element.47.values_ref, ...), custom_call_target="tpu_custom_call" | custom-call | flops 20000000 | tf_op jit(solution)/shard_map/pallas_call | solution.py:21
  37.1 2.9 %collective-permute-done.14.refs_3_ = bf16[2,3,512]{2,1,0:T(4,128)(2,1)S(1)} collective-permute-done((bf16[2,3,512]{2,1,0:T(4,128)(2,1)S(1)}, bf16[2,3,512]{2,1,0:T(4,128)(2,1)S(1)}, u32[]{:S(2)}, u32[]{:S(2)}) %collective-permute-start.14) | collective-permute-done | bytes 6176 | tf_op jit(solution)/shard_map/ppermute | solution.py:331
  40.0 0.8 %shard_map.211 = bf16[8,512]{1,0:T(8,128)(2,1)} custom-call(bf16[8,2048]{1,0:T(8,128)(2,1)S(1)} %get-tuple-element.33.residual_ref, f32[24,8]{1,0:T(8,128)S(1)} %get-tuple-element.34.mixing_ref, bf16[2,3,512]{2,1,0:T(4,128)(2,1)S(1)} %get-tuple-element.42.refs_0_, bf16[2,3,512]{2,1,0:T(4,128)(2,1)S(1)} %collective-permute-done.12.refs_1_, ...), custom_call_target="tpu_custom_call" | custom-call | flops 1000 | tf_op jit(solution)/shard_map/pallas_call | solution.py:21
  (20 shorter events, 2.7 us)
Async XLA Ops:
  3.0 5.4 %collective-permute-start.2 = (bf16[8,2048]{1,0:T(8,128)(2,1)S(1)}, bf16[8,2048]{1,0:T(8,128)(2,1)S(1)}, u32[]{:S(2)}, u32[]{:S(2)}) collective-permute-start(bf16[8,2048]{1,0:T(8,128)(2,1)S(1)} %get-tuple-element.29.tick_ref.refs_0_), channel_id=1, source_target_pairs={{0,3},{1,2},{2,1},{3,0},{4,7},{5,6},{6,5},{7,4},{8,11},{9,10},{10,... | collective-permute-start | bytes 98312 | tf_op jit(solution)/shard_map/ppermute | solution.py:331
  5.5 4.0 %collective-permute-start.1 = (bf16[8,2048]{1,0:T(8,128)(2,1)S(1)}, bf16[8,2048]{1,0:T(8,128)(2,1)S(1)}, u32[]{:S(2)}, u32[]{:S(2)}) collective-permute-start(bf16[8,2048]{1,0:T(8,128)(2,1)S(1)} %get-tuple-element.29.tick_ref.refs_0_), channel_id=1, source_target_pairs={{0,2},{1,3},{2,0},{3,1},{4,6},{5,7},{6,4},{7,5},{8,10},{9,11},{10,... | collective-permute-start | bytes 98312 | tf_op jit(solution)/shard_map/ppermute | solution.py:331
  6.2 3.3 %collective-permute-start = (bf16[8,2048]{1,0:T(8,128)(2,1)S(1)}, bf16[8,2048]{1,0:T(8,128)(2,1)S(1)}, u32[]{:S(2)}, u32[]{:S(2)}) collective-permute-start(bf16[8,2048]{1,0:T(8,128)(2,1)S(1)} %get-tuple-element.29.tick_ref.refs_0_), channel_id=1, source_target_pairs={{0,1},{1,0},{2,3},{3,2},{4,5},{5,4},{6,7},{7,6},{8,9},{9,8},{10,11... | collective-permute-start | bytes 98312 | tf_op jit(solution)/shard_map/ppermute | solution.py:331
  9.8 4.2 %collective-permute-start.3 = (bf16[4,6144]{1,0:T(4,128)(2,1)S(1)}, bf16[4,6144]{1,0:T(4,128)(2,1)S(1)}, u32[]{:S(2)}, u32[]{:S(2)}) collective-permute-start(bf16[4,6144]{1,0:T(4,128)(2,1)S(1)} %get-tuple-element.35.tick_ref), channel_id=1, source_target_pairs={{0,4},{4,0},{8,12},{12,8},{16,20},{20,16},{24,28},{28,24},{1,5},{5... | collective-permute-start | bytes 147464 | tf_op jit(solution)/shard_map/ppermute | solution.py:331
  14.1 4.2 %collective-permute-start.4 = (bf16[2,6144]{1,0:T(2,128)(2,1)S(1)}, bf16[2,6144]{1,0:T(2,128)(2,1)S(1)}, u32[]{:S(2)}, u32[]{:S(2)}) collective-permute-start(bf16[2,6144]{1,0:T(2,128)(2,1)S(1)} %get-tuple-element.38), channel_id=1, source_target_pairs={{0,8},{1,25},{2,10},{3,27},{4,12},{5,29},{6,14},{7,31},{8,0},{9,17... | collective-permute-start | bytes 73736 | tf_op jit(solution)/shard_map/ppermute | solution.py:341
  15.7 3.8 %collective-permute-start.5 = (bf16[2,6144]{1,0:T(2,128)(2,1)S(1)}, bf16[2,6144]{1,0:T(2,128)(2,1)S(1)}, u32[]{:S(2)}, u32[]{:S(2)}) collective-permute-start(bf16[2,6144]{1,0:T(2,128)(2,1)S(1)} %get-tuple-element.39), channel_id=1, source_target_pairs={{0,2},{1,17},{2,0},{3,19},{4,6},{5,21},{6,4},{7,23},{8,10},{9,25},... | collective-permute-start | bytes 73736 | tf_op jit(solution)/shard_map/ppermute | solution.py:341
  18.2 2.0 %collective-permute-start.6 = (bf16[2,6144]{1,0:T(2,128)(2,1)S(1)}, bf16[2,6144]{1,0:T(2,128)(2,1)S(1)}, u32[]{:S(2)}, u32[]{:S(2)}) collective-permute-start(bf16[2,6144]{1,0:T(2,128)(2,1)S(1)} %collective-permute-done.4.refs_1_), channel_id=1, source_target_pairs={{0,1},{1,0},{2,3},{3,2},{4,5},{5,4},{6,7},{7,6},{8,9},{9,8},{10,11... | collective-permute-start | bytes 73736 | tf_op jit(solution)/shard_map/ppermute | solution.py:331
  19.6 1.5 %collective-permute-start.7 = (bf16[2,6144]{1,0:T(2,128)(2,1)S(1)}, bf16[2,6144]{1,0:T(2,128)(2,1)S(1)}, u32[]{:S(2)}, u32[]{:S(2)}) collective-permute-start(bf16[2,6144]{1,0:T(2,128)(2,1)S(1)} %collective-permute-done.5.refs_2_), channel_id=1, source_target_pairs={{0,1},{1,0},{2,3},{3,2},{4,5},{5,4},{6,7},{7,6},{8,9},{9,8},{10,11... | collective-permute-start | bytes 73736 | tf_op jit(solution)/shard_map/ppermute | solution.py:331
  22.6 4.5 %collective-permute-start.10 = (bf16[24,1024]{1,0:T(8,128)(2,1)S(1)}, bf16[24,1024]{1,0:T(8,128)(2,1)S(1)}, u32[]{:S(2)}, u32[]{:S(2)}) collective-permute-start(bf16[24,1024]{1,0:T(8,128)(2,1)S(1)} %shard_map.206.tick_ref.near_ref), channel_id=1, source_target_pairs={{0,3},{1,2},{2,1},{3,0},{4,7},{5,6},{6,5},{7,4},{8,11},{9,10},{10,... | collective-permute-start | bytes 147464 | tf_op jit(solution)/shard_map/ppermute | solution.py:331
  23.9 4.1 %collective-permute-start.9 = (bf16[24,1024]{1,0:T(8,128)(2,1)S(1)}, bf16[24,1024]{1,0:T(8,128)(2,1)S(1)}, u32[]{:S(2)}, u32[]{:S(2)}) collective-permute-start(bf16[24,1024]{1,0:T(8,128)(2,1)S(1)} %shard_map.206.tick_ref.near_ref), channel_id=1, source_target_pairs={{0,2},{1,3},{2,0},{3,1},{4,6},{5,7},{6,4},{7,5},{8,10},{9,11},{10,... | collective-permute-start | bytes 147464 | tf_op jit(solution)/shard_map/ppermute | solution.py:331
  24.6 3.3 %collective-permute-start.8 = (bf16[24,1024]{1,0:T(8,128)(2,1)S(1)}, bf16[24,1024]{1,0:T(8,128)(2,1)S(1)}, u32[]{:S(2)}, u32[]{:S(2)}) collective-permute-start(bf16[24,1024]{1,0:T(8,128)(2,1)S(1)} %shard_map.206.tick_ref.near_ref), channel_id=1, source_target_pairs={{0,1},{1,0},{2,3},{3,2},{4,5},{5,4},{6,7},{7,6},{8,9},{9,8},{10,11... | collective-permute-start | bytes 147464 | tf_op jit(solution)/shard_map/ppermute | solution.py:331
  26.9 9.1 %copy-start = (f32[8,1,16384]{2,1,0:T(1,128)S(1)}, f32[8,1,16384]{2,1,0:T(1,128)}, u32[]{:S(2)}) copy-start(f32[8,1,16384]{2,1,0:T(1,128)} %param.27) | copy-start | bytes 1572868
  28.6 3.8 %collective-permute-start.11 = (bf16[4,3,512]{2,1,0:T(4,128)(2,1)S(1)}, bf16[4,3,512]{2,1,0:T(4,128)(2,1)S(1)}, u32[]{:S(2)}, u32[]{:S(2)}) collective-permute-start(bf16[4,3,512]{2,1,0:T(4,128)(2,1)S(1)} %get-tuple-element.41), channel_id=1, source_target_pairs={{0,4},{4,0},{8,12},{12,8},{16,20},{20,16},{24,28},{28,24},{1,5},{5... | collective-permute-start | bytes 36872 | tf_op jit(solution)/shard_map/ppermute | solution.py:331
  32.4 4.7 %collective-permute-start.13 = (bf16[2,3,512]{2,1,0:T(4,128)(2,1)S(1)}, bf16[2,3,512]{2,1,0:T(4,128)(2,1)S(1)}, u32[]{:S(2)}, u32[]{:S(2)}) collective-permute-start(bf16[2,3,512]{2,1,0:T(4,128)(2,1)S(1)} %get-tuple-element.44), channel_id=1, source_target_pairs={{0,16},{4,20},{8,24},{12,28},{16,0},{20,4},{24,8},{28,12},{1,17},{... | collective-permute-start | bytes 18440 | tf_op jit(solution)/shard_map/ppermute | solution.py:331
  34.6 5.4 %collective-permute-start.14 = (bf16[2,3,512]{2,1,0:T(4,128)(2,1)S(1)}, bf16[2,3,512]{2,1,0:T(4,128)(2,1)S(1)}, u32[]{:S(2)}, u32[]{:S(2)}) collective-permute-start(bf16[2,3,512]{2,1,0:T(4,128)(2,1)S(1)} %get-tuple-element.45), channel_id=1, source_target_pairs={{0,24},{4,28},{8,16},{12,20},{16,8},{20,12},{24,0},{28,4},{1,25},{... | collective-permute-start | bytes 18440 | tf_op jit(solution)/shard_map/ppermute | solution.py:331
  34.8 5.2 %collective-permute-start.12 = (bf16[2,3,512]{2,1,0:T(4,128)(2,1)S(1)}, bf16[2,3,512]{2,1,0:T(4,128)(2,1)S(1)}, u32[]{:S(2)}, u32[]{:S(2)}) collective-permute-start(bf16[2,3,512]{2,1,0:T(4,128)(2,1)S(1)} %get-tuple-element.43.tick_ref), channel_id=1, source_target_pairs={{0,8},{4,12},{8,0},{12,4},{16,24},{20,28},{24,16},{28,20},{1,9},{5... | collective-permute-start | bytes 18440 | tf_op jit(solution)/shard_map/ppermute | solution.py:331
where the time goes:
time: 41 us; the launch traced here: 40.8 us
  starting transfers between devices  14.6 us (36%)
  Pallas kernels  13.9 us (34%)
  waiting for transfers between devices  11.6 us (28%)
  between operations  0.72 us (2%)
    pallas_call x12, Pallas kernels, kernel_call(): pl.pallas_call(body, out_shape=outs, in_specs=in_specs or [VMEM] * len(in...  13.9 us
    ppermute x13, starting transfers between devices, swapped(): return lax.ppermute(value, axis, [(at, at ^ bits) for at in range(count)])  12 us
    ppermute x13, waiting for transfers between devices, swapped(): return lax.ppermute(value, axis, [(at, at ^ bits) for at in range(count)])  8.75 us
    ppermute x2, waiting for transfers between devices, sent(): return lax.ppermute(value, ('ep', 'tp'), pairs)  2.84 us
    ppermute x2, starting transfers between devices, sent(): return lax.ppermute(value, ('ep', 'tp'), pairs)  2.62 us
  transfers between devices with their start and end apart: 15, of which 8 were waited for; matrix products, arithmetic and copies ran while one was open for 0% of the time, Pallas kernels for 20%

commit v1 on v0

--- a/solution.py
+++ b/solution.py
@@ -7,6 +7,7 @@
 from jax.sharding import PartitionSpec as P
 
 FF = 4096
+LATEST = 2
 LANES = 128
 epsilon = 1e-06
 f32 = jnp.float32
@@ -278,15 +279,20 @@
     )
 
 
-def first_down_kernel(near_ref, weight_ref, total_ref):
-    total_ref[...] = down_term(near_ref, weight_ref, 0)
-
-
-def down_kernel(tp_count, total_ref, *refs):
-    hiddens, weight_ref, outs = refs[: tp_count - 1], refs[tp_count - 1], refs[tp_count:]
-    total = total_ref[...]
-    for k, hidden_ref in enumerate(hiddens):
-        total = total + down_term(hidden_ref, weight_ref, 1 + k)
+def first_down_kernel(own_ref, weight_ref, total_ref):
+    total_ref[...] = down_term(own_ref, weight_ref, 0)
+
+
+def next_down_kernel(numbers, before_ref, *refs):
+    *hiddens, weight_ref, total_ref = refs
+    total = before_ref[...]
+    for k, hidden_ref in zip(numbers, hiddens):
+        total = total + down_term(hidden_ref, weight_ref, k)
+    total_ref[...] = total
+
+
+def down_kernel(total_ref, hidden_ref, weight_ref, *outs):
+    total = total_ref[...] + down_term(hidden_ref, weight_ref, LATEST)
     if len(outs) == 1:
         spread(total, outs[0])
         return
@@ -312,13 +318,15 @@
     *parts, out_ref = refs
     width = out_ref.shape[1]
     start = pl.multiple_of(lax.axis_index("tp") * width, width)
-    routed = lax.dot_general(
-        mixing_ref[...],
-        stacked(parts),
-        (((0,), (0,)), ((), ())),
-        precision=lax.Precision.HIGHEST,
-        preferred_element_type=f32,
-    )
+    weights = mixing_ref[...].T
+    routed, at = None, 0
+    for ref in parts:
+        for place in range(ref.shape[0]):
+            block = ref[place].astype(f32)
+            for c in range(ref.shape[1]):
+                term = weights[:, at : at + 1] * block[c : c + 1, :]
+                routed = term if routed is None else routed + term
+                at += 1
     out_ref[...] = (residual_ref[:, pl.ds(start, width)].astype(f32) + routed).astype(bf16)
 
 
@@ -462,10 +470,18 @@
         cost=2_000_000,
         limit=8 << 20,
     )
+    middle = [k for k in reversed(range(1, tp_count)) if k != LATEST]
+    (total,) = kernel_call(
+        functools.partial(next_down_kernel, middle),
+        (pltpu.VMEM((rows, own_width), f32),),
+        (total, *(hiddens[k] for k in middle), down_w),
+        cost=2_000_000,
+        limit=8 << 20,
+    )
     blocks = kernel_call(
-        functools.partial(down_kernel, tp_count),
+        down_kernel,
         block_outs(own_width),
-        (total, *hiddens[1:], down_w),
+        (total, hiddens[LATEST], down_w),
         limit=8 << 20,
     )
 

time: 41 us -> 40.8 us (level)
  waiting for transfers between devices: 11.6 us -> 11.1 us
    ppermute x13, waiting for transfers between devices: 8.75 us -> 8.29 us  [swapped(): return lax.ppermute(value, axis, [(at, at ^ bits) for at in range(count)])]
    pallas_call x12 -> x13, Pallas kernels: 13.9 us -> 14 us  [kernel_call(): pl.pallas_call(body, out_shape=outs, in_specs=in_specs or [VMEM] * len(in...]
  transfers between devices with their start and end apart: 15 -> 15, of which waited for: 8 -> 8; matrix products, arithmetic and copies ran while one was open for 0% -> 0% of each run, Pallas kernels for 20% -> 21%
where the time goes in v1:
time: 40.8 us; the launch traced here: 40.6 us
  starting transfers between devices  14.8 us (36%)
  Pallas kernels  14 us (34%)
  waiting for transfers between devices  11.1 us (27%)
  between operations  0.73 us (2%)
    pallas_call x13, Pallas kernels, kernel_call(): pl.pallas_call(body, out_shape=outs, in_specs=in_specs or [VMEM] * len(in...  14 us
    ppermute x13, starting transfers between devices, swapped(): return lax.ppermute(value, axis, [(at, at ^ bits) for at in range(count)])  12.2 us
    ppermute x13, waiting for transfers between devices, swapped(): return lax.ppermute(value, axis, [(at, at ^ bits) for at in range(count)])  8.29 us
    ppermute x2, waiting for transfers between devices, sent(): return lax.ppermute(value, ('ep', 'tp'), pairs)  2.84 us
    ppermute x2, starting transfers between devices, sent(): return lax.ppermute(value, ('ep', 'tp'), pairs)  2.62 us
  transfers between devices with their start and end apart: 15, of which 8 were waited for; matrix products, arithmetic and copies ran while one was open for 0% of the time, Pallas kernels for 21%

profile of v1, /device:TPU:0, one launch (start us, length us, event | category | flops | bytes accessed | tf_op | source)
XLA Modules:
  0.0 40.6 jit_solution(7841111505129290576)
XLA Ops:
  0.6 2.4 %shard_map.201 = (bf16[8,2048]{1,0:T(8,128)(2,1)S(1)}, f32[8,128]{1,0:T(8,128)S(1)}, f32[8,128]{1,0:T(8,128)S(1)}, f32[8,128]{1,0:T(8,128)S(1)}, f32[8,128]{1,0:...) custom-call(bf16[8,2048]{1,0:T(8,128)(2,1)} %tokens_hbm.1, ...), custom_call_target="tpu_custom_call" | custom-call | flops 1000 | tf_op jit(solution)/shard_map/pallas_call | solution.py:22
  3.0 2.5 %collective-permute-start.2 = (bf16[8,2048]{1,0:T(8,128)(2,1)S(1)}, bf16[8,2048]{1,0:T(8,128)(2,1)S(1)}, u32[]{:S(2)}, u32[]{:S(2)}) collective-permute-start(bf16[8,2048]{1,0:T(8,128)(2,1)S(1)} %get-tuple-element.29.tick_ref.refs_0_), channel_id=1, source_target_pairs={{0,3},{1,2},{2,1},{3,0},{4,7},{5,6},{6,5},{7,4},{8,11},{9,10},{10,... | collective-permute-start | bytes 98312 | tf_op jit(solution)/shard_map/ppermute | solution.py:339
  5.5 0.6 %collective-permute-start.1 = (bf16[8,2048]{1,0:T(8,128)(2,1)S(1)}, bf16[8,2048]{1,0:T(8,128)(2,1)S(1)}, u32[]{:S(2)}, u32[]{:S(2)}) collective-permute-start(bf16[8,2048]{1,0:T(8,128)(2,1)S(1)} %get-tuple-element.29.tick_ref.refs_0_), channel_id=1, source_target_pairs={{0,2},{1,3},{2,0},{3,1},{4,6},{5,7},{6,4},{7,5},{8,10},{9,11},{10,... | collective-permute-start | bytes 98312 | tf_op jit(solution)/shard_map/ppermute | solution.py:339
  6.2 2.2 %shard_map.202.tick_ref.refs_5_ = bf16[2048,1024]{1,0:T(8,128)(2,1)S(1)} custom-call(bf16[8,2048]{1,0:T(8,128)(2,1)S(1)} %get-tuple-element.29.tick_ref.refs_0_, bf16[2048,1024]{1,0:T(8,128)(2,1)} %source_ref.3), custom_call_target="tpu_custom_call" | custom-call | flops 20000000 | tf_op jit(solution)/shard_map/pallas_call | solution.py:22
  8.5 1.1 %collective-permute-done.1.refs_2_ = bf16[8,2048]{1,0:T(8,128)(2,1)S(1)} collective-permute-done((bf16[8,2048]{1,0:T(8,128)(2,1)S(1)}, bf16[8,2048]{1,0:T(8,128)(2,1)S(1)}, u32[]{:S(2)}, u32[]{:S(2)}) %collective-permute-start.1) | collective-permute-done | bytes 32800 | tf_op jit(solution)/shard_map/ppermute | solution.py:339
  9.8 1.6 %collective-permute-start.3 = (bf16[4,6144]{1,0:T(4,128)(2,1)S(1)}, bf16[4,6144]{1,0:T(4,128)(2,1)S(1)}, u32[]{:S(2)}, u32[]{:S(2)}) collective-permute-start(bf16[4,6144]{1,0:T(4,128)(2,1)S(1)} %get-tuple-element.35.tick_ref), channel_id=1, source_target_pairs={{0,4},{4,0},{8,12},{12,8},{16,20},{20,16},{24,28},{28,24},{1,5},{5... | collective-permute-start | bytes 147464 | tf_op jit(solution)/shard_map/ppermute | solution.py:339
  11.4 2.2 %shard_map.204.tick_ref.refs_6_ = bf16[2048,1024]{1,0:T(8,128)(2,1)S(1)} custom-call(bf16[4,6144]{1,0:T(4,128)(2,1)S(1)} %get-tuple-element.35.tick_ref, bf16[2048,1024]{1,0:T(8,128)(2,1)} %source_ref.4), custom_call_target="tpu_custom_call" | custom-call | flops 20000000 | tf_op jit(solution)/shard_map/pallas_call | solution.py:22
  14.1 1.6 %collective-permute-start.4 = (bf16[2,6144]{1,0:T(2,128)(2,1)S(1)}, bf16[2,6144]{1,0:T(2,128)(2,1)S(1)}, u32[]{:S(2)}, u32[]{:S(2)}) collective-permute-start(bf16[2,6144]{1,0:T(2,128)(2,1)S(1)} %get-tuple-element.38), channel_id=1, source_target_pairs={{0,8},{1,25},{2,10},{3,27},{4,12},{5,29},{6,14},{7,31},{8,0},{9,17... | collective-permute-start | bytes 73736 | tf_op jit(solution)/shard_map/ppermute | solution.py:349
  15.7 1.0 %collective-permute-start.5 = (bf16[2,6144]{1,0:T(2,128)(2,1)S(1)}, bf16[2,6144]{1,0:T(2,128)(2,1)S(1)}, u32[]{:S(2)}, u32[]{:S(2)}) collective-permute-start(bf16[2,6144]{1,0:T(2,128)(2,1)S(1)} %get-tuple-element.39), channel_id=1, source_target_pairs={{0,2},{1,17},{2,0},{3,19},{4,6},{5,21},{6,4},{7,23},{8,10},{9,25},... | collective-permute-start | bytes 73736 | tf_op jit(solution)/shard_map/ppermute | solution.py:349
  16.7 1.5 %collective-permute-done.4.refs_1_ = bf16[2,6144]{1,0:T(2,128)(2,1)S(1)} collective-permute-done((bf16[2,6144]{1,0:T(2,128)(2,1)S(1)}, bf16[2,6144]{1,0:T(2,128)(2,1)S(1)}, u32[]{:S(2)}, u32[]{:S(2)}) %collective-permute-start.4) | collective-permute-done | bytes 24608 | tf_op jit(solution)/shard_map/ppermute | solution.py:349
  18.2 1.3 %collective-permute-done.5.refs_2_ = bf16[2,6144]{1,0:T(2,128)(2,1)S(1)} collective-permute-done((bf16[2,6144]{1,0:T(2,128)(2,1)S(1)}, bf16[2,6144]{1,0:T(2,128)(2,1)S(1)}, u32[]{:S(2)}, u32[]{:S(2)}) %collective-permute-start.5) | collective-permute-done | bytes 24608 | tf_op jit(solution)/shard_map/ppermute | solution.py:349
  19.6 0.7 %collective-permute-start.7 = (bf16[2,6144]{1,0:T(2,128)(2,1)S(1)}, bf16[2,6144]{1,0:T(2,128)(2,1)S(1)}, u32[]{:S(2)}, u32[]{:S(2)}) collective-permute-start(bf16[2,6144]{1,0:T(2,128)(2,1)S(1)} %collective-permute-done.5.refs_2_), channel_id=1, source_target_pairs={{0,1},{1,0},{2,3},{3,2},{4,5},{5,4},{6,7},{7,6},{8,9},{9,8},{10,11... | collective-permute-start | bytes 73736 | tf_op jit(solution)/shard_map/ppermute | solution.py:339
  20.2 0.8 %collective-permute-done.7.refs_4_ = bf16[2,6144]{1,0:T(2,128)(2,1)S(1)} collective-permute-done((bf16[2,6144]{1,0:T(2,128)(2,1)S(1)}, bf16[2,6144]{1,0:T(2,128)(2,1)S(1)}, u32[]{:S(2)}, u32[]{:S(2)}) %collective-permute-start.7) | collective-permute-done | bytes 24608 | tf_op jit(solution)/shard_map/ppermute | solution.py:339
  21.1 1.6 %shard_map.206.tick_ref.own_ref = bf16[24,1024]{1,0:T(8,128)(2,1)S(1)} custom-call(bf16[2,6144]{1,0:T(2,128)(2,1)S(1)} %get-tuple-element.37.refs_0_, bf16[2,6144]{1,0:T(2,128)(2,1)S(1)} %collective-permute-done.4.refs_1_, bf16[2,6144]{1,0:T(2,128)(2,1)S(1)} %collective-permute-done.5.refs_2_, bf16[2,6144]{1,0:T(2,128)(2,1)S(1)} %collective-permute-done.6.refs_3_, ...), custom_call_target="tpu_custom_call" | custom-call | flops 1000 | tf_op jit(solution)/shard_map/pallas_call | solution.py:22
  23.0 1.0 %collective-permute-start.8 = (bf16[24,1024]{1,0:T(8,128)(2,1)S(1)}, bf16[24,1024]{1,0:T(8,128)(2,1)S(1)}, u32[]{:S(2)}, u32[]{:S(2)}) collective-permute-start(bf16[24,1024]{1,0:T(8,128)(2,1)S(1)} %shard_map.206.tick_ref.own_ref), channel_id=1, source_target_pairs={{0,3},{1,2},{2,1},{3,0},{4,7},{5,6},{6,5},{7,4},{8,11},{9,10},{10,... | collective-permute-start | bytes 147464 | tf_op jit(solution)/shard_map/ppermute | solution.py:339
  24.0 0.8 %collective-permute-start.10 = (bf16[24,1024]{1,0:T(8,128)(2,1)S(1)}, bf16[24,1024]{1,0:T(8,128)(2,1)S(1)}, u32[]{:S(2)}, u32[]{:S(2)}) collective-permute-start(bf16[24,1024]{1,0:T(8,128)(2,1)S(1)} %shard_map.206.tick_ref.own_ref), channel_id=1, source_target_pairs={{0,2},{1,3},{2,0},{3,1},{4,6},{5,7},{6,4},{7,5},{8,10},{9,11},{10,... | collective-permute-start | bytes 147464 | tf_op jit(solution)/shard_map/ppermute | solution.py:339
  24.8 2.2 %shard_map.207.weight_ref.refs_2_ = bf16[4096,512]{1,0:T(8,128)(2,1)S(1)} custom-call(bf16[24,1024]{1,0:T(8,128)(2,1)S(1)} %shard_map.206.tick_ref.own_ref, bf16[4096,512]{1,0:T(8,128)(2,1)} %source_ref.5), custom_call_target="tpu_custom_call" | custom-call | flops 20000000 | tf_op jit(solution)/shard_map/pallas_call | solution.py:22
  28.4 1.1 %collective-permute-start.11 = (bf16[4,3,512]{2,1,0:T(4,128)(2,1)S(1)}, bf16[4,3,512]{2,1,0:T(4,128)(2,1)S(1)}, u32[]{:S(2)}, u32[]{:S(2)}) collective-permute-start(bf16[4,3,512]{2,1,0:T(4,128)(2,1)S(1)} %get-tuple-element.41), channel_id=1, source_target_pairs={{0,4},{4,0},{8,12},{12,8},{16,20},{20,16},{24,28},{28,24},{1,5},{5... | collective-permute-start | bytes 36872 | tf_op jit(solution)/shard_map/ppermute | solution.py:339
  29.5 2.8 %collective-permute-done.11.far_ref = bf16[4,3,512]{2,1,0:T(4,128)(2,1)S(1)} collective-permute-done((bf16[4,3,512]{2,1,0:T(4,128)(2,1)S(1)}, bf16[4,3,512]{2,1,0:T(4,128)(2,1)S(1)}, u32[]{:S(2)}, u32[]{:S(2)}) %collective-permute-start.11) | collective-permute-done | bytes 12320 | tf_op jit(solution)/shard_map/ppermute | solution.py:339
  32.3 2.1 %collective-permute-start.13 = (bf16[2,3,512]{2,1,0:T(4,128)(2,1)S(1)}, bf16[2,3,512]{2,1,0:T(4,128)(2,1)S(1)}, u32[]{:S(2)}, u32[]{:S(2)}) collective-permute-start(bf16[2,3,512]{2,1,0:T(4,128)(2,1)S(1)} %get-tuple-element.44), channel_id=1, source_target_pairs={{0,16},{4,20},{8,24},{12,28},{16,0},{20,4},{24,8},{28,12},{1,17},{... | collective-permute-start | bytes 18440 | tf_op jit(solution)/shard_map/ppermute | solution.py:339
  34.6 1.2 %collective-permute-start.12 = (bf16[2,3,512]{2,1,0:T(4,128)(2,1)S(1)}, bf16[2,3,512]{2,1,0:T(4,128)(2,1)S(1)}, u32[]{:S(2)}, u32[]{:S(2)}) collective-permute-start(bf16[2,3,512]{2,1,0:T(4,128)(2,1)S(1)} %get-tuple-element.43.tick_ref), channel_id=1, source_target_pairs={{0,8},{4,12},{8,0},{12,4},{16,24},{20,28},{24,16},{28,20},{1,9},{5... | collective-permute-start | bytes 18440 | tf_op jit(solution)/shard_map/ppermute | solution.py:339
  35.8 1.1 %shard_map.213 = (f32[8,128,128]{2,1,0:T(8,128)}, f32[8,128]{1,0:T(8,128)}, f32[1,8]{1,0:T(1,128)}) custom-call(bf16[2,3,512]{2,1,0:T(4,128)(2,1)S(1)} %get-tuple-element.43.tick_ref, f32[8,128,128]{2,1,0:T(8,128)S(1)} %bitcast.12, f32[8,128]{1,0:T(8,128)S(1)} %get-tuple-element.46.keys_ref, f32[8,128]{1,0:T(8,128)S(1)} %get-tuple-element.47.values_ref, ...), custom_call_target="tpu_custom_call" | custom-call | flops 20000000 | tf_op jit(solution)/shard_map/pallas_call | solution.py:22
  36.9 2.9 %collective-permute-done.14.refs_3_ = bf16[2,3,512]{2,1,0:T(4,128)(2,1)S(1)} collective-permute-done((bf16[2,3,512]{2,1,0:T(4,128)(2,1)S(1)}, bf16[2,3,512]{2,1,0:T(4,128)(2,1)S(1)}, u32[]{:S(2)}, u32[]{:S(2)}) %collective-permute-start.14) | collective-permute-done | bytes 6176 | tf_op jit(solution)/shard_map/ppermute | solution.py:339
  39.8 0.8 %shard_map.212 = bf16[8,512]{1,0:T(8,128)(2,1)} custom-call(bf16[8,2048]{1,0:T(8,128)(2,1)S(1)} %get-tuple-element.33.residual_ref, f32[24,8]{1,0:T(8,128)S(1)} %get-tuple-element.34.mixing_ref, bf16[2,3,512]{2,1,0:T(4,128)(2,1)S(1)} %get-tuple-element.42.refs_0_, bf16[2,3,512]{2,1,0:T(4,128)(2,1)S(1)} %collective-permute-done.12.refs_1_, ...), custom_call_target="tpu_custom_call" | custom-call | flops 1000 | tf_op jit(solution)/shard_map/pallas_call | solution.py:22
  (21 shorter events, 2.8 us)
Async XLA Ops:
  3.0 5.4 %collective-permute-start.2 = (bf16[8,2048]{1,0:T(8,128)(2,1)S(1)}, bf16[8,2048]{1,0:T(8,128)(2,1)S(1)}, u32[]{:S(2)}, u32[]{:S(2)}) collective-permute-start(bf16[8,2048]{1,0:T(8,128)(2,1)S(1)} %get-tuple-element.29.tick_ref.refs_0_), channel_id=1, source_target_pairs={{0,3},{1,2},{2,1},{3,0},{4,7},{5,6},{6,5},{7,4},{8,11},{9,10},{10,... | collective-permute-start | bytes 98312 | tf_op jit(solution)/shard_map/ppermute | solution.py:339
  5.5 4.0 %collective-permute-start.1 = (bf16[8,2048]{1,0:T(8,128)(2,1)S(1)}, bf16[8,2048]{1,0:T(8,128)(2,1)S(1)}, u32[]{:S(2)}, u32[]{:S(2)}) collective-permute-start(bf16[8,2048]{1,0:T(8,128)(2,1)S(1)} %get-tuple-element.29.tick_ref.refs_0_), channel_id=1, source_target_pairs={{0,2},{1,3},{2,0},{3,1},{4,6},{5,7},{6,4},{7,5},{8,10},{9,11},{10,... | collective-permute-start | bytes 98312 | tf_op jit(solution)/shard_map/ppermute | solution.py:339
  6.2 3.3 %collective-permute-start = (bf16[8,2048]{1,0:T(8,128)(2,1)S(1)}, bf16[8,2048]{1,0:T(8,128)(2,1)S(1)}, u32[]{:S(2)}, u32[]{:S(2)}) collective-permute-start(bf16[8,2048]{1,0:T(8,128)(2,1)S(1)} %get-tuple-element.29.tick_ref.refs_0_), channel_id=1, source_target_pairs={{0,1},{1,0},{2,3},{3,2},{4,5},{5,4},{6,7},{7,6},{8,9},{9,8},{10,11... | collective-permute-start | bytes 98312 | tf_op jit(solution)/shard_map/ppermute | solution.py:339
  9.8 4.2 %collective-permute-start.3 = (bf16[4,6144]{1,0:T(4,128)(2,1)S(1)}, bf16[4,6144]{1,0:T(4,128)(2,1)S(1)}, u32[]{:S(2)}, u32[]{:S(2)}) collective-permute-start(bf16[4,6144]{1,0:T(4,128)(2,1)S(1)} %get-tuple-element.35.tick_ref), channel_id=1, source_target_pairs={{0,4},{4,0},{8,12},{12,8},{16,20},{20,16},{24,28},{28,24},{1,5},{5... | collective-permute-start | bytes 147464 | tf_op jit(solution)/shard_map/ppermute | solution.py:339
  14.1 4.2 %collective-permute-start.4 = (bf16[2,6144]{1,0:T(2,128)(2,1)S(1)}, bf16[2,6144]{1,0:T(2,128)(2,1)S(1)}, u32[]{:S(2)}, u32[]{:S(2)}) collective-permute-start(bf16[2,6144]{1,0:T(2,128)(2,1)S(1)} %get-tuple-element.38), channel_id=1, source_target_pairs={{0,8},{1,25},{2,10},{3,27},{4,12},{5,29},{6,14},{7,31},{8,0},{9,17... | collective-permute-start | bytes 73736 | tf_op jit(solution)/shard_map/ppermute | solution.py:349
  15.7 3.8 %collective-permute-start.5 = (bf16[2,6144]{1,0:T(2,128)(2,1)S(1)}, bf16[2,6144]{1,0:T(2,128)(2,1)S(1)}, u32[]{:S(2)}, u32[]{:S(2)}) collective-permute-start(bf16[2,6144]{1,0:T(2,128)(2,1)S(1)} %get-tuple-element.39), channel_id=1, source_target_pairs={{0,2},{1,17},{2,0},{3,19},{4,6},{5,21},{6,4},{7,23},{8,10},{9,25},... | collective-permute-start | bytes 73736 | tf_op jit(solution)/shard_map/ppermute | solution.py:349
  18.2 2.0 %collective-permute-start.6 = (bf16[2,6144]{1,0:T(2,128)(2,1)S(1)}, bf16[2,6144]{1,0:T(2,128)(2,1)S(1)}, u32[]{:S(2)}, u32[]{:S(2)}) collective-permute-start(bf16[2,6144]{1,0:T(2,128)(2,1)S(1)} %collective-permute-done.4.refs_1_), channel_id=1, source_target_pairs={{0,1},{1,0},{2,3},{3,2},{4,5},{5,4},{6,7},{7,6},{8,9},{9,8},{10,11... | collective-permute-start | bytes 73736 | tf_op jit(solution)/shard_map/ppermute | solution.py:339
  19.6 1.5 %collective-permute-start.7 = (bf16[2,6144]{1,0:T(2,128)(2,1)S(1)}, bf16[2,6144]{1,0:T(2,128)(2,1)S(1)}, u32[]{:S(2)}, u32[]{:S(2)}) collective-permute-start(bf16[2,6144]{1,0:T(2,128)(2,1)S(1)} %collective-permute-done.5.refs_2_), channel_id=1, source_target_pairs={{0,1},{1,0},{2,3},{3,2},{4,5},{5,4},{6,7},{7,6},{8,9},{9,8},{10,11... | collective-permute-start | bytes 73736 | tf_op jit(solution)/shard_map/ppermute | solution.py:339
  22.6 4.7 %collective-permute-start.9 = (bf16[24,1024]{1,0:T(8,128)(2,1)S(1)}, bf16[24,1024]{1,0:T(8,128)(2,1)S(1)}, u32[]{:S(2)}, u32[]{:S(2)}) collective-permute-start(bf16[24,1024]{1,0:T(8,128)(2,1)S(1)} %shard_map.206.tick_ref.own_ref), channel_id=1, source_target_pairs={{0,1},{1,0},{2,3},{3,2},{4,5},{5,4},{6,7},{7,6},{8,9},{9,8},{10,11... | collective-permute-start | bytes 147464 | tf_op jit(solution)/shard_map/ppermute | solution.py:339
  23.0 4.3 %collective-permute-start.8 = (bf16[24,1024]{1,0:T(8,128)(2,1)S(1)}, bf16[24,1024]{1,0:T(8,128)(2,1)S(1)}, u32[]{:S(2)}, u32[]{:S(2)}) collective-permute-start(bf16[24,1024]{1,0:T(8,128)(2,1)S(1)} %shard_map.206.tick_ref.own_ref), channel_id=1, source_target_pairs={{0,3},{1,2},{2,1},{3,0},{4,7},{5,6},{6,5},{7,4},{8,11},{9,10},{10,... | collective-permute-start | bytes 147464 | tf_op jit(solution)/shard_map/ppermute | solution.py:339
  24.0 4.1 %collective-permute-start.10 = (bf16[24,1024]{1,0:T(8,128)(2,1)S(1)}, bf16[24,1024]{1,0:T(8,128)(2,1)S(1)}, u32[]{:S(2)}, u32[]{:S(2)}) collective-permute-start(bf16[24,1024]{1,0:T(8,128)(2,1)S(1)} %shard_map.206.tick_ref.own_ref), channel_id=1, source_target_pairs={{0,2},{1,3},{2,0},{3,1},{4,6},{5,7},{6,4},{7,5},{8,10},{9,11},{10,... | collective-permute-start | bytes 147464 | tf_op jit(solution)/shard_map/ppermute | solution.py:339
  27.3 8.5 %copy-start = (f32[8,1,16384]{2,1,0:T(1,128)S(1)}, f32[8,1,16384]{2,1,0:T(1,128)}, u32[]{:S(2)}) copy-start(f32[8,1,16384]{2,1,0:T(1,128)} %param.27) | copy-start | bytes 1572868
  28.4 3.8 %collective-permute-start.11 = (bf16[4,3,512]{2,1,0:T(4,128)(2,1)S(1)}, bf16[4,3,512]{2,1,0:T(4,128)(2,1)S(1)}, u32[]{:S(2)}, u32[]{:S(2)}) collective-permute-start(bf16[4,3,512]{2,1,0:T(4,128)(2,1)S(1)} %get-tuple-element.41), channel_id=1, source_target_pairs={{0,4},{4,0},{8,12},{12,8},{16,20},{20,16},{24,28},{28,24},{1,5},{5... | collective-permute-start | bytes 36872 | tf_op jit(solution)/shard_map/ppermute | solution.py:339
  32.3 4.7 %collective-permute-start.13 = (bf16[2,3,512]{2,1,0:T(4,128)(2,1)S(1)}, bf16[2,3,512]{2,1,0:T(4,128)(2,1)S(1)}, u32[]{:S(2)}, u32[]{:S(2)}) collective-permute-start(bf16[2,3,512]{2,1,0:T(4,128)(2,1)S(1)} %get-tuple-element.44), channel_id=1, source_target_pairs={{0,16},{4,20},{8,24},{12,28},{16,0},{20,4},{24,8},{28,12},{1,17},{... | collective-permute-start | bytes 18440 | tf_op jit(solution)/shard_map/ppermute | solution.py:339
  34.4 5.4 %collective-permute-start.14 = (bf16[2,3,512]{2,1,0:T(4,128)(2,1)S(1)}, bf16[2,3,512]{2,1,0:T(4,128)(2,1)S(1)}, u32[]{:S(2)}, u32[]{:S(2)}) collective-permute-start(bf16[2,3,512]{2,1,0:T(4,128)(2,1)S(1)} %get-tuple-element.45), channel_id=1, source_target_pairs={{0,24},{4,28},{8,16},{12,20},{16,8},{20,12},{24,0},{28,4},{1,25},{... | collective-permute-start | bytes 18440 | tf_op jit(solution)/shard_map/ppermute | solution.py:339
  34.6 5.2 %collective-permute-start.12 = (bf16[2,3,512]{2,1,0:T(4,128)(2,1)S(1)}, bf16[2,3,512]{2,1,0:T(4,128)(2,1)S(1)}, u32[]{:S(2)}, u32[]{:S(2)}) collective-permute-start(bf16[2,3,512]{2,1,0:T(4,128)(2,1)S(1)} %get-tuple-element.43.tick_ref), channel_id=1, source_target_pairs={{0,8},{4,12},{8,0},{12,4},{16,24},{20,28},{24,16},{28,20},{1,9},{5... | collective-permute-start | bytes 18440 | tf_op jit(solution)/shard_map/ppermute | solution.py:339

commit v2 on v1

--- a/solution.py
+++ b/solution.py
@@ -252,13 +252,13 @@
     if len(parts) == 1:
         rows = stacked(parts).astype(bf16)
     else:
-        own, first, second, other_first, other_second = [ref[...].astype(f32) for ref in parts]
+        own, first, second, other_first = [ref[...].astype(f32) for ref in parts]
         odd = lax.axis_index("tp") & 1 == 1
         pieces = []
         for part in (
             own,
             jnp.where(odd, other_first, first),
-            jnp.where(odd, second, other_second),
+            second,
             jnp.where(odd, first, other_first),
         ):
             pieces += [part[:, at : at + deep] for at in range(0, part.shape[1], deep)]
@@ -366,9 +366,8 @@
         limit=4 << 20,
     )
     first = sent(first, lambda e, t: (e ^ 6, t) if t & 1 else (e ^ 2, t))
-    second = sent(second, lambda e, t: (e ^ 4, t) if t & 1 else (e, t ^ 2))
-    shared = [swapped(part, "tp", 1) for part in (first, second)]
-    return [own, first, second, *shared], up_w
+    second = sent(second, lambda e, t: (e ^ 4, t))
+    return [own, first, second, swapped(first, "tp", 1)], up_w
 
 
 def returned_blocks(near, far):

time: 40.8 us -> 40.5 us (level)
  waiting for transfers between devices: 11.1 us -> 9.62 us
  starting transfers between devices: 14.8 us -> 16 us
    ppermute x2, starting transfers between devices: 2.62 us -> 4.23 us  [sent(): return lax.ppermute(value, ('ep', 'tp'), pairs)]
    ppermute x13 -> x12, waiting for transfers between devices: 8.29 us -> 7.09 us  [swapped(): return lax.ppermute(value, axis, [(at, at ^ bits) for at in range(count)])]
    ppermute x13 -> x12, starting transfers between devices: 12.2 us -> 11.8 us  [swapped(): return lax.ppermute(value, axis, [(at, at ^ bits) for at in range(count)])]
  transfers between devices with their start and end apart: 15 -> 14, of which waited for: 8 -> 6; matrix products, arithmetic and copies ran while one was open for 0% -> 0% of each run, Pallas kernels for 21% -> 21%
where the time goes in v2:
time: 40.5 us; the launch traced here: 40.3 us
  starting transfers between devices  16 us (40%)
  Pallas kernels  14 us (35%)
  waiting for transfers between devices  9.62 us (24%)
  between operations  0.73 us (2%)
    pallas_call x13, Pallas kernels, kernel_call(): pl.pallas_call(body, out_shape=outs, in_specs=in_specs or [VMEM] * len(in...  14 us
    ppermute x12, starting transfers between devices, swapped(): return lax.ppermute(value, axis, [(at, at ^ bits) for at in range(count)])  11.8 us
    ppermute x12, waiting for transfers between devices, swapped(): return lax.ppermute(value, axis, [(at, at ^ bits) for at in range(count)])  7.09 us
    ppermute x2, starting transfers between devices, sent(): return lax.ppermute(value, ('ep', 'tp'), pairs)  4.23 us
    ppermute x2, waiting for transfers between devices, sent(): return lax.ppermute(value, ('ep', 'tp'), pairs)  2.54 us
  transfers between devices with their start and end apart: 14, of which 6 were waited for; matrix products, arithmetic and copies ran while one was open for 0% of the time, Pallas kernels for 21%

profile of v2, /device:TPU:0, one launch (start us, length us, event | category | flops | bytes accessed | tf_op | source)
XLA Modules:
  0.0 40.3 jit_solution(9734284140001063119)
XLA Ops:
  0.6 2.4 %shard_map.201 = (bf16[8,2048]{1,0:T(8,128)(2,1)S(1)}, f32[8,128]{1,0:T(8,128)S(1)}, f32[8,128]{1,0:T(8,128)S(1)}, f32[8,128]{1,0:T(8,128)S(1)}, f32[8,128]{1,0:...) custom-call(bf16[8,2048]{1,0:T(8,128)(2,1)} %tokens_hbm.1, ...), custom_call_target="tpu_custom_call" | custom-call | flops 1000 | tf_op jit(solution)/shard_map/pallas_call | solution.py:22
  3.0 2.5 %collective-permute-start.2 = (bf16[8,2048]{1,0:T(8,128)(2,1)S(1)}, bf16[8,2048]{1,0:T(8,128)(2,1)S(1)}, u32[]{:S(2)}, u32[]{:S(2)}) collective-permute-start(bf16[8,2048]{1,0:T(8,128)(2,1)S(1)} %get-tuple-element.29.tick_ref.refs_0_), channel_id=1, source_target_pairs={{0,3},{1,2},{2,1},{3,0},{4,7},{5,6},{6,5},{7,4},{8,11},{9,10},{10,... | collective-permute-start | bytes 98312 | tf_op jit(solution)/shard_map/ppermute | solution.py:339
  5.5 0.6 %collective-permute-start.1 = (bf16[8,2048]{1,0:T(8,128)(2,1)S(1)}, bf16[8,2048]{1,0:T(8,128)(2,1)S(1)}, u32[]{:S(2)}, u32[]{:S(2)}) collective-permute-start(bf16[8,2048]{1,0:T(8,128)(2,1)S(1)} %get-tuple-element.29.tick_ref.refs_0_), channel_id=1, source_target_pairs={{0,2},{1,3},{2,0},{3,1},{4,6},{5,7},{6,4},{7,5},{8,10},{9,11},{10,... | collective-permute-start | bytes 98312 | tf_op jit(solution)/shard_map/ppermute | solution.py:339
  6.2 2.2 %shard_map.202.tick_ref.refs_4_ = bf16[2048,1024]{1,0:T(8,128)(2,1)S(1)} custom-call(bf16[8,2048]{1,0:T(8,128)(2,1)S(1)} %get-tuple-element.29.tick_ref.refs_0_, bf16[2048,1024]{1,0:T(8,128)(2,1)} %source_ref.3), custom_call_target="tpu_custom_call" | custom-call | flops 20000000 | tf_op jit(solution)/shard_map/pallas_call | solution.py:22
  8.5 1.1 %collective-permute-done.1.refs_2_ = bf16[8,2048]{1,0:T(8,128)(2,1)S(1)} collective-permute-done((bf16[8,2048]{1,0:T(8,128)(2,1)S(1)}, bf16[8,2048]{1,0:T(8,128)(2,1)S(1)}, u32[]{:S(2)}, u32[]{:S(2)}) %collective-permute-start.1) | collective-permute-done | bytes 32800 | tf_op jit(solution)/shard_map/ppermute | solution.py:339
  9.8 1.6 %collective-permute-start.3 = (bf16[4,6144]{1,0:T(4,128)(2,1)S(1)}, bf16[4,6144]{1,0:T(4,128)(2,1)S(1)}, u32[]{:S(2)}, u32[]{:S(2)}) collective-permute-start(bf16[4,6144]{1,0:T(4,128)(2,1)S(1)} %get-tuple-element.35.tick_ref), channel_id=1, source_target_pairs={{0,4},{4,0},{8,12},{12,8},{16,20},{20,16},{24,28},{28,24},{1,5},{5... | collective-permute-start | bytes 147464 | tf_op jit(solution)/shard_map/ppermute | solution.py:339
  11.4 2.2 %shard_map.204.tick_ref.refs_5_ = bf16[2048,1024]{1,0:T(8,128)(2,1)S(1)} custom-call(bf16[4,6144]{1,0:T(4,128)(2,1)S(1)} %get-tuple-element.35.tick_ref, bf16[2048,1024]{1,0:T(8,128)(2,1)} %source_ref.4), custom_call_target="tpu_custom_call" | custom-call | flops 20000000 | tf_op jit(solution)/shard_map/pallas_call | solution.py:22
  13.6 0.4 collective-permute-done.3.far_ref
  14.1 1.6 %collective-permute-start.4 = (bf16[2,6144]{1,0:T(2,128)(2,1)S(1)}, bf16[2,6144]{1,0:T(2,128)(2,1)S(1)}, u32[]{:S(2)}, u32[]{:S(2)}) collective-permute-start(bf16[2,6144]{1,0:T(2,128)(2,1)S(1)} %get-tuple-element.38), channel_id=1, source_target_pairs={{0,8},{1,25},{2,10},{3,27},{4,12},{5,29},{6,14},{7,31},{8,0},{9,17... | collective-permute-start | bytes 73736 | tf_op jit(solution)/shard_map/ppermute | solution.py:349
  15.7 2.6 %collective-permute-start.5 = (bf16[2,6144]{1,0:T(2,128)(2,1)S(1)}, bf16[2,6144]{1,0:T(2,128)(2,1)S(1)}, u32[]{:S(2)}, u32[]{:S(2)}) collective-permute-start(bf16[2,6144]{1,0:T(2,128)(2,1)S(1)} %get-tuple-element.39), channel_id=1, source_target_pairs={{0,16},{1,17},{2,18},{3,19},{4,20},{5,21},{6,22},{7,23},{8,24},{9,... | collective-permute-start | bytes 73736 | tf_op jit(solution)/shard_map/ppermute | solution.py:349
  18.3 2.5 %collective-permute-done.5.refs_2_ = bf16[2,6144]{1,0:T(2,128)(2,1)S(1)} collective-permute-done((bf16[2,6144]{1,0:T(2,128)(2,1)S(1)}, bf16[2,6144]{1,0:T(2,128)(2,1)S(1)}, u32[]{:S(2)}, u32[]{:S(2)}) %collective-permute-start.5) | collective-permute-done | bytes 24608 | tf_op jit(solution)/shard_map/ppermute | solution.py:349
  20.9 1.5 %shard_map.206.tick_ref.own_ref = bf16[24,1024]{1,0:T(8,128)(2,1)S(1)} custom-call(bf16[2,6144]{1,0:T(2,128)(2,1)S(1)} %get-tuple-element.37.refs_0_, bf16[2,6144]{1,0:T(2,128)(2,1)S(1)} %collective-permute-done.4.refs_1_, bf16[2,6144]{1,0:T(2,128)(2,1)S(1)} %collective-permute-done.5.refs_2_, bf16[2,6144]{1,0:T(2,128)(2,1)S(1)} %collective-permute-done.6.refs_3_, ...), custom_call_target="tpu_custom_call" | custom-call | flops 1000 | tf_op jit(solution)/shard_map/pallas_call | solution.py:22
  22.6 0.9 %collective-permute-start.7 = (bf16[24,1024]{1,0:T(8,128)(2,1)S(1)}, bf16[24,1024]{1,0:T(8,128)(2,1)S(1)}, u32[]{:S(2)}, u32[]{:S(2)}) collective-permute-start(bf16[24,1024]{1,0:T(8,128)(2,1)S(1)} %shard_map.206.tick_ref.own_ref), channel_id=1, source_target_pairs={{0,3},{1,2},{2,1},{3,0},{4,7},{5,6},{6,5},{7,4},{8,11},{9,10},{10,... | collective-permute-start | bytes 147464 | tf_op jit(solution)/shard_map/ppermute | solution.py:339
  23.4 1.1 %collective-permute-start.9 = (bf16[24,1024]{1,0:T(8,128)(2,1)S(1)}, bf16[24,1024]{1,0:T(8,128)(2,1)S(1)}, u32[]{:S(2)}, u32[]{:S(2)}) collective-permute-start(bf16[24,1024]{1,0:T(8,128)(2,1)S(1)} %shard_map.206.tick_ref.own_ref), channel_id=1, source_target_pairs={{0,2},{1,3},{2,0},{3,1},{4,6},{5,7},{6,4},{7,5},{8,10},{9,11},{10,... | collective-permute-start | bytes 147464 | tf_op jit(solution)/shard_map/ppermute | solution.py:339
  24.6 2.2 %shard_map.207.weight_ref.refs_2_ = bf16[4096,512]{1,0:T(8,128)(2,1)S(1)} custom-call(bf16[24,1024]{1,0:T(8,128)(2,1)S(1)} %shard_map.206.tick_ref.own_ref, bf16[4096,512]{1,0:T(8,128)(2,1)} %source_ref.5), custom_call_target="tpu_custom_call" | custom-call | flops 20000000 | tf_op jit(solution)/shard_map/pallas_call | solution.py:22
  27.1 0.5 %shard_map.209.total_ref = f32[24,512]{1,0:T(8,128)S(1)} custom-call(f32[24,512]{1,0:T(8,128)S(1)} %shard_map.208.before_ref, bf16[24,1024]{1,0:T(8,128)(2,1)S(1)} %collective-permute-done.7.refs_0_, bf16[24,1024]{1,0:T(8,128)(2,1)S(1)} %collective-permute-done.8.refs_1_, bf16[4096,512]{1,0:T(8,128)(2,1)S(1)} %shard_map.207.weight_ref.refs_2_), custom_call_target="tpu_custom_call" | custom-call | flops 2000000 | tf_op jit(solution)/shard_map/pallas_call | solution.py:22
  27.7 0.3 shard_map.210
  28.0 1.3 %collective-permute-start.10 = (bf16[4,3,512]{2,1,0:T(4,128)(2,1)S(1)}, bf16[4,3,512]{2,1,0:T(4,128)(2,1)S(1)}, u32[]{:S(2)}, u32[]{:S(2)}) collective-permute-start(bf16[4,3,512]{2,1,0:T(4,128)(2,1)S(1)} %get-tuple-element.41), channel_id=1, source_target_pairs={{0,4},{4,0},{8,12},{12,8},{16,20},{20,16},{24,28},{28,24},{1,5},{5... | collective-permute-start | bytes 36872 | tf_op jit(solution)/shard_map/ppermute | solution.py:339
  29.3 2.5 %collective-permute-done.10.far_ref = bf16[4,3,512]{2,1,0:T(4,128)(2,1)S(1)} collective-permute-done((bf16[4,3,512]{2,1,0:T(4,128)(2,1)S(1)}, bf16[4,3,512]{2,1,0:T(4,128)(2,1)S(1)}, u32[]{:S(2)}, u32[]{:S(2)}) %collective-permute-start.10) | collective-permute-done | bytes 12320 | tf_op jit(solution)/shard_map/ppermute | solution.py:339
  31.8 2.2 %collective-permute-start.12 = (bf16[2,3,512]{2,1,0:T(4,128)(2,1)S(1)}, bf16[2,3,512]{2,1,0:T(4,128)(2,1)S(1)}, u32[]{:S(2)}, u32[]{:S(2)}) collective-permute-start(bf16[2,3,512]{2,1,0:T(4,128)(2,1)S(1)} %get-tuple-element.44), channel_id=1, source_target_pairs={{0,16},{4,20},{8,24},{12,28},{16,0},{20,4},{24,8},{28,12},{1,17},{... | collective-permute-start | bytes 18440 | tf_op jit(solution)/shard_map/ppermute | solution.py:339
  34.3 1.1 %collective-permute-start.11 = (bf16[2,3,512]{2,1,0:T(4,128)(2,1)S(1)}, bf16[2,3,512]{2,1,0:T(4,128)(2,1)S(1)}, u32[]{:S(2)}, u32[]{:S(2)}) collective-permute-start(bf16[2,3,512]{2,1,0:T(4,128)(2,1)S(1)} %get-tuple-element.43.tick_ref), channel_id=1, source_target_pairs={{0,8},{4,12},{8,0},{12,4},{16,24},{20,28},{24,16},{28,20},{1,9},{5... | collective-permute-start | bytes 18440 | tf_op jit(solution)/shard_map/ppermute | solution.py:339
  35.4 1.1 %shard_map.213 = (f32[8,128,128]{2,1,0:T(8,128)}, f32[8,128]{1,0:T(8,128)}, f32[1,8]{1,0:T(1,128)}) custom-call(bf16[2,3,512]{2,1,0:T(4,128)(2,1)S(1)} %get-tuple-element.43.tick_ref, f32[8,128,128]{2,1,0:T(8,128)S(1)} %bitcast.12, f32[8,128]{1,0:T(8,128)S(1)} %get-tuple-element.46.keys_ref, f32[8,128]{1,0:T(8,128)S(1)} %get-tuple-element.47.values_ref, ...), custom_call_target="tpu_custom_call" | custom-call | flops 20000000 | tf_op jit(solution)/shard_map/pallas_call | solution.py:22
  36.5 3.0 %collective-permute-done.13.refs_3_ = bf16[2,3,512]{2,1,0:T(4,128)(2,1)S(1)} collective-permute-done((bf16[2,3,512]{2,1,0:T(4,128)(2,1)S(1)}, bf16[2,3,512]{2,1,0:T(4,128)(2,1)S(1)}, u32[]{:S(2)}, u32[]{:S(2)}) %collective-permute-start.13) | collective-permute-done | bytes 6176 | tf_op jit(solution)/shard_map/ppermute | solution.py:339
  39.5 0.8 %shard_map.212 = bf16[8,512]{1,0:T(8,128)(2,1)} custom-call(bf16[8,2048]{1,0:T(8,128)(2,1)S(1)} %get-tuple-element.33.residual_ref, f32[24,8]{1,0:T(8,128)S(1)} %get-tuple-element.34.mixing_ref, bf16[2,3,512]{2,1,0:T(4,128)(2,1)S(1)} %get-tuple-element.42.refs_0_, bf16[2,3,512]{2,1,0:T(4,128)(2,1)S(1)} %collective-permute-done.11.refs_1_, ...), custom_call_target="tpu_custom_call" | custom-call | flops 1000 | tf_op jit(solution)/shard_map/pallas_call | solution.py:22
  (19 shorter events, 1.3 us)
Async XLA Ops:
  3.0 5.4 %collective-permute-start.2 = (bf16[8,2048]{1,0:T(8,128)(2,1)S(1)}, bf16[8,2048]{1,0:T(8,128)(2,1)S(1)}, u32[]{:S(2)}, u32[]{:S(2)}) collective-permute-start(bf16[8,2048]{1,0:T(8,128)(2,1)S(1)} %get-tuple-element.29.tick_ref.refs_0_), channel_id=1, source_target_pairs={{0,3},{1,2},{2,1},{3,0},{4,7},{5,6},{6,5},{7,4},{8,11},{9,10},{10,... | collective-permute-start | bytes 98312 | tf_op jit(solution)/shard_map/ppermute | solution.py:339
  5.5 4.0 %collective-permute-start.1 = (bf16[8,2048]{1,0:T(8,128)(2,1)S(1)}, bf16[8,2048]{1,0:T(8,128)(2,1)S(1)}, u32[]{:S(2)}, u32[]{:S(2)}) collective-permute-start(bf16[8,2048]{1,0:T(8,128)(2,1)S(1)} %get-tuple-element.29.tick_ref.refs_0_), channel_id=1, source_target_pairs={{0,2},{1,3},{2,0},{3,1},{4,6},{5,7},{6,4},{7,5},{8,10},{9,11},{10,... | collective-permute-start | bytes 98312 | tf_op jit(solution)/shard_map/ppermute | solution.py:339
  6.2 3.3 %collective-permute-start = (bf16[8,2048]{1,0:T(8,128)(2,1)S(1)}, bf16[8,2048]{1,0:T(8,128)(2,1)S(1)}, u32[]{:S(2)}, u32[]{:S(2)}) collective-permute-start(bf16[8,2048]{1,0:T(8,128)(2,1)S(1)} %get-tuple-element.29.tick_ref.refs_0_), channel_id=1, source_target_pairs={{0,1},{1,0},{2,3},{3,2},{4,5},{5,4},{6,7},{7,6},{8,9},{9,8},{10,11... | collective-permute-start | bytes 98312 | tf_op jit(solution)/shard_map/ppermute | solution.py:339
  9.8 4.2 %collective-permute-start.3 = (bf16[4,6144]{1,0:T(4,128)(2,1)S(1)}, bf16[4,6144]{1,0:T(4,128)(2,1)S(1)}, u32[]{:S(2)}, u32[]{:S(2)}) collective-permute-start(bf16[4,6144]{1,0:T(4,128)(2,1)S(1)} %get-tuple-element.35.tick_ref), channel_id=1, source_target_pairs={{0,4},{4,0},{8,12},{12,8},{16,20},{20,16},{24,28},{28,24},{1,5},{5... | collective-permute-start | bytes 147464 | tf_op jit(solution)/shard_map/ppermute | solution.py:339
  14.1 4.2 %collective-permute-start.4 = (bf16[2,6144]{1,0:T(2,128)(2,1)S(1)}, bf16[2,6144]{1,0:T(2,128)(2,1)S(1)}, u32[]{:S(2)}, u32[]{:S(2)}) collective-permute-start(bf16[2,6144]{1,0:T(2,128)(2,1)S(1)} %get-tuple-element.38), channel_id=1, source_target_pairs={{0,8},{1,25},{2,10},{3,27},{4,12},{5,29},{6,14},{7,31},{8,0},{9,17... | collective-permute-start | bytes 73736 | tf_op jit(solution)/shard_map/ppermute | solution.py:349
  15.7 5.1 %collective-permute-start.5 = (bf16[2,6144]{1,0:T(2,128)(2,1)S(1)}, bf16[2,6144]{1,0:T(2,128)(2,1)S(1)}, u32[]{:S(2)}, u32[]{:S(2)}) collective-permute-start(bf16[2,6144]{1,0:T(2,128)(2,1)S(1)} %get-tuple-element.39), channel_id=1, source_target_pairs={{0,16},{1,17},{2,18},{3,19},{4,20},{5,21},{6,22},{7,23},{8,24},{9,... | collective-permute-start | bytes 73736 | tf_op jit(solution)/shard_map/ppermute | solution.py:349
  18.3 2.5 %collective-permute-start.6 = (bf16[2,6144]{1,0:T(2,128)(2,1)S(1)}, bf16[2,6144]{1,0:T(2,128)(2,1)S(1)}, u32[]{:S(2)}, u32[]{:S(2)}) collective-permute-start(bf16[2,6144]{1,0:T(2,128)(2,1)S(1)} %collective-permute-done.4.refs_1_), channel_id=1, source_target_pairs={{0,1},{1,0},{2,3},{3,2},{4,5},{5,4},{6,7},{7,6},{8,9},{9,8},{10,11... | collective-permute-start | bytes 73736 | tf_op jit(solution)/shard_map/ppermute | solution.py:339
  22.4 4.7 %collective-permute-start.8 = (bf16[24,1024]{1,0:T(8,128)(2,1)S(1)}, bf16[24,1024]{1,0:T(8,128)(2,1)S(1)}, u32[]{:S(2)}, u32[]{:S(2)}) collective-permute-start(bf16[24,1024]{1,0:T(8,128)(2,1)S(1)} %shard_map.206.tick_ref.own_ref), channel_id=1, source_target_pairs={{0,1},{1,0},{2,3},{3,2},{4,5},{5,4},{6,7},{7,6},{8,9},{9,8},{10,11... | collective-permute-start | bytes 147464 | tf_op jit(solution)/shard_map/ppermute | solution.py:339
  22.6 4.6 %collective-permute-start.7 = (bf16[24,1024]{1,0:T(8,128)(2,1)S(1)}, bf16[24,1024]{1,0:T(8,128)(2,1)S(1)}, u32[]{:S(2)}, u32[]{:S(2)}) collective-permute-start(bf16[24,1024]{1,0:T(8,128)(2,1)S(1)} %shard_map.206.tick_ref.own_ref), channel_id=1, source_target_pairs={{0,3},{1,2},{2,1},{3,0},{4,7},{5,6},{6,5},{7,4},{8,11},{9,10},{10,... | collective-permute-start | bytes 147464 | tf_op jit(solution)/shard_map/ppermute | solution.py:339
  23.4 4.2 %collective-permute-start.9 = (bf16[24,1024]{1,0:T(8,128)(2,1)S(1)}, bf16[24,1024]{1,0:T(8,128)(2,1)S(1)}, u32[]{:S(2)}, u32[]{:S(2)}) collective-permute-start(bf16[24,1024]{1,0:T(8,128)(2,1)S(1)} %shard_map.206.tick_ref.own_ref), channel_id=1, source_target_pairs={{0,2},{1,3},{2,0},{3,1},{4,6},{5,7},{6,4},{7,5},{8,10},{9,11},{10,... | collective-permute-start | bytes 147464 | tf_op jit(solution)/shard_map/ppermute | solution.py:339
  27.1 8.3 %copy-start = (f32[8,1,16384]{2,1,0:T(1,128)S(1)}, f32[8,1,16384]{2,1,0:T(1,128)}, u32[]{:S(2)}) copy-start(f32[8,1,16384]{2,1,0:T(1,128)} %param.27) | copy-start | bytes 1572868
  28.0 3.8 %collective-permute-start.10 = (bf16[4,3,512]{2,1,0:T(4,128)(2,1)S(1)}, bf16[4,3,512]{2,1,0:T(4,128)(2,1)S(1)}, u32[]{:S(2)}, u32[]{:S(2)}) collective-permute-start(bf16[4,3,512]{2,1,0:T(4,128)(2,1)S(1)} %get-tuple-element.41), channel_id=1, source_target_pairs={{0,4},{4,0},{8,12},{12,8},{16,20},{20,16},{24,28},{28,24},{1,5},{5... | collective-permute-start | bytes 36872 | tf_op jit(solution)/shard_map/ppermute | solution.py:339
  31.8 4.7 %collective-permute-start.12 = (bf16[2,3,512]{2,1,0:T(4,128)(2,1)S(1)}, bf16[2,3,512]{2,1,0:T(4,128)(2,1)S(1)}, u32[]{:S(2)}, u32[]{:S(2)}) collective-permute-start(bf16[2,3,512]{2,1,0:T(4,128)(2,1)S(1)} %get-tuple-element.44), channel_id=1, source_target_pairs={{0,16},{4,20},{8,24},{12,28},{16,0},{20,4},{24,8},{28,12},{1,17},{... | collective-permute-start | bytes 18440 | tf_op jit(solution)/shard_map/ppermute | solution.py:339
  34.1 5.4 %collective-permute-start.13 = (bf16[2,3,512]{2,1,0:T(4,128)(2,1)S(1)}, bf16[2,3,512]{2,1,0:T(4,128)(2,1)S(1)}, u32[]{:S(2)}, u32[]{:S(2)}) collective-permute-start(bf16[2,3,512]{2,1,0:T(4,128)(2,1)S(1)} %get-tuple-element.45), channel_id=1, source_target_pairs={{0,24},{4,28},{8,16},{12,20},{16,8},{20,12},{24,0},{28,4},{1,25},{... | collective-permute-start | bytes 18440 | tf_op jit(solution)/shard_map/ppermute | solution.py:339
  34.3 5.2 %collective-permute-start.11 = (bf16[2,3,512]{2,1,0:T(4,128)(2,1)S(1)}, bf16[2,3,512]{2,1,0:T(4,128)(2,1)S(1)}, u32[]{:S(2)}, u32[]{:S(2)}) collective-permute-start(bf16[2,3,512]{2,1,0:T(4,128)(2,1)S(1)} %get-tuple-element.43.tick_ref), channel_id=1, source_target_pairs={{0,8},{4,12},{8,0},{12,4},{16,24},{20,28},{24,16},{28,20},{1,9},{5... | collective-permute-start | bytes 18440 | tf_op jit(solution)/shard_map/ppermute | solution.py:339

commit v3 on v2

--- a/solution.py
+++ b/solution.py
@@ -96,7 +96,7 @@
     pairs = (
         (tokens_hbm, tokens_ref), (gain_hbm, gain_ref), (ids_hbm, ids_ref), (weights_hbm, weights_ref),
         (wi_hbm, wi_ref), (wf_hbm, wf_ref), (bias_hbm, bias_ref), (max_hbm, max_ref), (norm_hbm, norm_ref),
-        (wk_hbm, wk_ref), (wq_hbm, wq_ref), (mem_hbm, mem_ref), (wv_hbm, wv_ref), (wo_hbm, wo_ref),
+        (wk_hbm, wk_ref), (wq_hbm, wq_ref), (wv_hbm, wv_ref), (mem_hbm, mem_ref), (wo_hbm, wo_ref),
         (next_gain_hbm, next_gain_ref),
     )
     copies = [pltpu.make_async_copy(a, b, sems.at[i]) for i, (a, b) in enumerate(pairs)]
@@ -153,13 +153,13 @@
     denominator = jnp.sum(query * new_norm, 1, keepdims=True)
     scale = jnp.maximum(jnp.abs(denominator), jnp.exp(-new_max))
     arrive(11, 12)
+    value = project(wv_ref)
+    values_ref[...] = value
+    arrive(12, 13)
     read = []
     for s in range(seq_count):
         read.append(jnp.sum(mem_ref[s] * query_t[:, s : s + 1], 0, keepdims=True))
     read = jnp.concatenate(read, 0)
-    arrive(12, 13)
-    value = project(wv_ref)
-    values_ref[...] = value
     readout = (keep * read + (fresh * match) * value) / scale
     arrive(13, 14)
     partial_ref[...] = jnp.dot(
@@ -314,20 +314,37 @@
         )
 
 
-def final_kernel(residual_ref, mixing_ref, *refs):
+def weighted(mixing_ref, parts):
+    weights = mixing_ref[...].T
+    total = None
+    for number, ref in parts:
+        count, slots, _ = ref.shape
+        for place in range(count):
+            block = ref[place].astype(f32)
+            for c in range(slots):
+                at = (number * count + place) * slots + c
+                term = weights[:, at : at + 1] * block[c : c + 1, :]
+                total = term if total is None else total + term
+    return total
+
+
+def early_kernel(numbers, residual_ref, mixing_ref, *refs):
     *parts, out_ref = refs
     width = out_ref.shape[1]
     start = pl.multiple_of(lax.axis_index("tp") * width, width)
-    weights = mixing_ref[...].T
-    routed, at = None, 0
-    for ref in parts:
-        for place in range(ref.shape[0]):
-            block = ref[place].astype(f32)
-            for c in range(ref.shape[1]):
-                term = weights[:, at : at + 1] * block[c : c + 1, :]
-                routed = term if routed is None else routed + term
-                at += 1
-    out_ref[...] = (residual_ref[:, pl.ds(start, width)].astype(f32) + routed).astype(bf16)
+    residual = residual_ref[:, pl.ds(start, width)].astype(f32)
+    out_ref[...] = residual + weighted(mixing_ref, zip(numbers, parts))
+
+
+def final_kernel(number, before_ref, mixing_ref, part_ref, out_ref):
+    out_ref[...] = (before_ref[...] + weighted(mixing_ref, [(number, part_ref)])).astype(bf16)
+
+
+def whole_kernel(residual_ref, mixing_ref, part_ref, out_ref):
+    width = out_ref.shape[1]
+    start = pl.multiple_of(lax.axis_index("tp") * width, width)
+    residual = residual_ref[:, pl.ds(start, width)].astype(f32)
+    out_ref[...] = (residual + weighted(mixing_ref, [(0, part_ref)])).astype(bf16)
 
 
 def in_hbm(*values):
@@ -504,12 +521,27 @@
         tick = blocks[0]
         returned = [lax.all_to_all(tick, "ep", split_axis=0, concat_axis=0, tiled=True)]
     new_memory, new_norm, new_max = state(tick)
-    (out_tokens,) = kernel_call(
-        final_kernel,
-        (struct((seq_count, own_width), bf16),),
-        (residual, mixing, *returned),
-        limit=8 << 20,
-    )
+    out_struct = struct((seq_count, own_width), bf16)
+    if direct:
+        last = 1
+        numbers = [k for k in range(len(returned)) if k != last]
+        (before,) = kernel_call(
+            functools.partial(early_kernel, numbers),
+            (pltpu.VMEM(out_struct.shape, f32),),
+            (residual, mixing, *(returned[k] for k in numbers)),
+            cost=2_000_000,
+            limit=8 << 20,
+        )
+        (out_tokens,) = kernel_call(
+            functools.partial(final_kernel, last),
+            (out_struct,),
+            (before, mixing, returned[last]),
+            limit=8 << 20,
+        )
+    else:
+        (out_tokens,) = kernel_call(
+            whole_kernel, (out_struct,), (residual, mixing, *returned), limit=8 << 20
+        )
     return (
         out_tokens,
         new_memory.reshape(mem_state.shape),

time: 40.5 us -> 40.6 us (level)
    pallas_call x13 -> x14, Pallas kernels: 14 us -> 14.1 us  [kernel_call(): pl.pallas_call(body, out_shape=outs, in_specs=in_specs or [VMEM] * len(in...]
where the time goes in v3:
time: 40.6 us; the launch traced here: 40.5 us
  starting transfers between devices  16 us (39%)
  Pallas kernels  14.1 us (35%)
  waiting for transfers between devices  9.63 us (24%)
  between operations  0.74 us (2%)
    pallas_call x14, Pallas kernels, kernel_call(): pl.pallas_call(body, out_shape=outs, in_specs=in_specs or [VMEM] * len(in...  14.1 us
    ppermute x12, starting transfers between devices, swapped(): return lax.ppermute(value, axis, [(at, at ^ bits) for at in range(count)])  11.8 us
    ppermute x12, waiting for transfers between devices, swapped(): return lax.ppermute(value, axis, [(at, at ^ bits) for at in range(count)])  7.09 us
    ppermute x2, starting transfers between devices, sent(): return lax.ppermute(value, ('ep', 'tp'), pairs)  4.23 us
    ppermute x2, waiting for transfers between devices, sent(): return lax.ppermute(value, ('ep', 'tp'), pairs)  2.54 us
  transfers between devices with their start and end apart: 14, of which 6 were waited for; matrix products, arithmetic and copies ran while one was open for 0% of the time, Pallas kernels for 21%

profile of v3, /device:TPU:0, one launch (start us, length us, event | category | flops | bytes accessed | tf_op | source)
XLA Modules:
  0.0 40.5 jit_solution(14796202415989992541)
XLA Ops:
  0.6 2.4 %shard_map.201 = (bf16[8,2048]{1,0:T(8,128)(2,1)S(1)}, f32[8,128]{1,0:T(8,128)S(1)}, f32[8,128]{1,0:T(8,128)S(1)}, f32[8,128]{1,0:T(8,128)S(1)}, f32[8,128]{1,0:...) custom-call(bf16[8,2048]{1,0:T(8,128)(2,1)} %tokens_hbm.1, ...), custom_call_target="tpu_custom_call" | custom-call | flops 1000 | tf_op jit(solution)/shard_map/pallas_call | solution.py:22
  3.0 2.5 %collective-permute-start.2 = (bf16[8,2048]{1,0:T(8,128)(2,1)S(1)}, bf16[8,2048]{1,0:T(8,128)(2,1)S(1)}, u32[]{:S(2)}, u32[]{:S(2)}) collective-permute-start(bf16[8,2048]{1,0:T(8,128)(2,1)S(1)} %get-tuple-element.29.tick_ref.refs_0_), channel_id=1, source_target_pairs={{0,3},{1,2},{2,1},{3,0},{4,7},{5,6},{6,5},{7,4},{8,11},{9,10},{10,... | collective-permute-start | bytes 98312 | tf_op jit(solution)/shard_map/ppermute | solution.py:356
  5.5 0.6 %collective-permute-start.1 = (bf16[8,2048]{1,0:T(8,128)(2,1)S(1)}, bf16[8,2048]{1,0:T(8,128)(2,1)S(1)}, u32[]{:S(2)}, u32[]{:S(2)}) collective-permute-start(bf16[8,2048]{1,0:T(8,128)(2,1)S(1)} %get-tuple-element.29.tick_ref.refs_0_), channel_id=1, source_target_pairs={{0,2},{1,3},{2,0},{3,1},{4,6},{5,7},{6,4},{7,5},{8,10},{9,11},{10,... | collective-permute-start | bytes 98312 | tf_op jit(solution)/shard_map/ppermute | solution.py:356
  6.2 2.2 %shard_map.202.tick_ref.refs_4_ = bf16[2048,1024]{1,0:T(8,128)(2,1)S(1)} custom-call(bf16[8,2048]{1,0:T(8,128)(2,1)S(1)} %get-tuple-element.29.tick_ref.refs_0_, bf16[2048,1024]{1,0:T(8,128)(2,1)} %source_ref.3), custom_call_target="tpu_custom_call" | custom-call | flops 20000000 | tf_op jit(solution)/shard_map/pallas_call | solution.py:22
  8.5 1.1 %collective-permute-done.1.refs_2_ = bf16[8,2048]{1,0:T(8,128)(2,1)S(1)} collective-permute-done((bf16[8,2048]{1,0:T(8,128)(2,1)S(1)}, bf16[8,2048]{1,0:T(8,128)(2,1)S(1)}, u32[]{:S(2)}, u32[]{:S(2)}) %collective-permute-start.1) | collective-permute-done | bytes 32800 | tf_op jit(solution)/shard_map/ppermute | solution.py:356
  9.8 1.6 %collective-permute-start.3 = (bf16[4,6144]{1,0:T(4,128)(2,1)S(1)}, bf16[4,6144]{1,0:T(4,128)(2,1)S(1)}, u32[]{:S(2)}, u32[]{:S(2)}) collective-permute-start(bf16[4,6144]{1,0:T(4,128)(2,1)S(1)} %get-tuple-element.35.tick_ref), channel_id=1, source_target_pairs={{0,4},{4,0},{8,12},{12,8},{16,20},{20,16},{24,28},{28,24},{1,5},{5... | collective-permute-start | bytes 147464 | tf_op jit(solution)/shard_map/ppermute | solution.py:356
  11.4 2.2 %shard_map.204.tick_ref.refs_5_ = bf16[2048,1024]{1,0:T(8,128)(2,1)S(1)} custom-call(bf16[4,6144]{1,0:T(4,128)(2,1)S(1)} %get-tuple-element.35.tick_ref, bf16[2048,1024]{1,0:T(8,128)(2,1)} %source_ref.4), custom_call_target="tpu_custom_call" | custom-call | flops 20000000 | tf_op jit(solution)/shard_map/pallas_call | solution.py:22
  13.6 0.4 collective-permute-done.3.far_ref
  14.1 1.6 %collective-permute-start.4 = (bf16[2,6144]{1,0:T(2,128)(2,1)S(1)}, bf16[2,6144]{1,0:T(2,128)(2,1)S(1)}, u32[]{:S(2)}, u32[]{:S(2)}) collective-permute-start(bf16[2,6144]{1,0:T(2,128)(2,1)S(1)} %get-tuple-element.38), channel_id=1, source_target_pairs={{0,8},{1,25},{2,10},{3,27},{4,12},{5,29},{6,14},{7,31},{8,0},{9,17... | collective-permute-start | bytes 73736 | tf_op jit(solution)/shard_map/ppermute | solution.py:366
  15.7 2.6 %collective-permute-start.5 = (bf16[2,6144]{1,0:T(2,128)(2,1)S(1)}, bf16[2,6144]{1,0:T(2,128)(2,1)S(1)}, u32[]{:S(2)}, u32[]{:S(2)}) collective-permute-start(bf16[2,6144]{1,0:T(2,128)(2,1)S(1)} %get-tuple-element.39), channel_id=1, source_target_pairs={{0,16},{1,17},{2,18},{3,19},{4,20},{5,21},{6,22},{7,23},{8,24},{9,... | collective-permute-start | bytes 73736 | tf_op jit(solution)/shard_map/ppermute | solution.py:366
  18.3 2.5 %collective-permute-done.5.refs_2_ = bf16[2,6144]{1,0:T(2,128)(2,1)S(1)} collective-permute-done((bf16[2,6144]{1,0:T(2,128)(2,1)S(1)}, bf16[2,6144]{1,0:T(2,128)(2,1)S(1)}, u32[]{:S(2)}, u32[]{:S(2)}) %collective-permute-start.5) | collective-permute-done | bytes 24608 | tf_op jit(solution)/shard_map/ppermute | solution.py:366
  20.9 1.5 %shard_map.206.tick_ref.own_ref = bf16[24,1024]{1,0:T(8,128)(2,1)S(1)} custom-call(bf16[2,6144]{1,0:T(2,128)(2,1)S(1)} %get-tuple-element.37.refs_0_, bf16[2,6144]{1,0:T(2,128)(2,1)S(1)} %collective-permute-done.4.refs_1_, bf16[2,6144]{1,0:T(2,128)(2,1)S(1)} %collective-permute-done.5.refs_2_, bf16[2,6144]{1,0:T(2,128)(2,1)S(1)} %collective-permute-done.6.refs_3_, ...), custom_call_target="tpu_custom_call" | custom-call | flops 1000 | tf_op jit(solution)/shard_map/pallas_call | solution.py:22
  22.6 0.9 %collective-permute-start.7 = (bf16[24,1024]{1,0:T(8,128)(2,1)S(1)}, bf16[24,1024]{1,0:T(8,128)(2,1)S(1)}, u32[]{:S(2)}, u32[]{:S(2)}) collective-permute-start(bf16[24,1024]{1,0:T(8,128)(2,1)S(1)} %shard_map.206.tick_ref.own_ref), channel_id=1, source_target_pairs={{0,3},{1,2},{2,1},{3,0},{4,7},{5,6},{6,5},{7,4},{8,11},{9,10},{10,... | collective-permute-start | bytes 147464 | tf_op jit(solution)/shard_map/ppermute | solution.py:356
  23.4 1.1 %collective-permute-start.9 = (bf16[24,1024]{1,0:T(8,128)(2,1)S(1)}, bf16[24,1024]{1,0:T(8,128)(2,1)S(1)}, u32[]{:S(2)}, u32[]{:S(2)}) collective-permute-start(bf16[24,1024]{1,0:T(8,128)(2,1)S(1)} %shard_map.206.tick_ref.own_ref), channel_id=1, source_target_pairs={{0,2},{1,3},{2,0},{3,1},{4,6},{5,7},{6,4},{7,5},{8,10},{9,11},{10,... | collective-permute-start | bytes 147464 | tf_op jit(solution)/shard_map/ppermute | solution.py:356
  24.6 2.2 %shard_map.207.weight_ref.refs_2_ = bf16[4096,512]{1,0:T(8,128)(2,1)S(1)} custom-call(bf16[24,1024]{1,0:T(8,128)(2,1)S(1)} %shard_map.206.tick_ref.own_ref, bf16[4096,512]{1,0:T(8,128)(2,1)} %source_ref.5), custom_call_target="tpu_custom_call" | custom-call | flops 20000000 | tf_op jit(solution)/shard_map/pallas_call | solution.py:22
  27.1 0.5 %shard_map.209.total_ref = f32[24,512]{1,0:T(8,128)S(1)} custom-call(f32[24,512]{1,0:T(8,128)S(1)} %shard_map.208.before_ref, bf16[24,1024]{1,0:T(8,128)(2,1)S(1)} %collective-permute-done.7.refs_0_, bf16[24,1024]{1,0:T(8,128)(2,1)S(1)} %collective-permute-done.8.refs_1_, bf16[4096,512]{1,0:T(8,128)(2,1)S(1)} %shard_map.207.weight_ref.refs_2_), custom_call_target="tpu_custom_call" | custom-call | flops 2000000 | tf_op jit(solution)/shard_map/pallas_call | solution.py:22
  27.7 0.3 shard_map.210
  28.0 1.3 %collective-permute-start.10 = (bf16[4,3,512]{2,1,0:T(4,128)(2,1)S(1)}, bf16[4,3,512]{2,1,0:T(4,128)(2,1)S(1)}, u32[]{:S(2)}, u32[]{:S(2)}) collective-permute-start(bf16[4,3,512]{2,1,0:T(4,128)(2,1)S(1)} %get-tuple-element.41), channel_id=1, source_target_pairs={{0,4},{4,0},{8,12},{12,8},{16,20},{20,16},{24,28},{28,24},{1,5},{5... | collective-permute-start | bytes 36872 | tf_op jit(solution)/shard_map/ppermute | solution.py:356
  29.3 2.5 %collective-permute-done.10.far_ref = bf16[4,3,512]{2,1,0:T(4,128)(2,1)S(1)} collective-permute-done((bf16[4,3,512]{2,1,0:T(4,128)(2,1)S(1)}, bf16[4,3,512]{2,1,0:T(4,128)(2,1)S(1)}, u32[]{:S(2)}, u32[]{:S(2)}) %collective-permute-start.10) | collective-permute-done | bytes 12320 | tf_op jit(solution)/shard_map/ppermute | solution.py:356
  31.8 2.2 %collective-permute-start.11 = (bf16[2,3,512]{2,1,0:T(4,128)(2,1)S(1)}, bf16[2,3,512]{2,1,0:T(4,128)(2,1)S(1)}, u32[]{:S(2)}, u32[]{:S(2)}) collective-permute-start(bf16[2,3,512]{2,1,0:T(4,128)(2,1)S(1)} %get-tuple-element.43), channel_id=1, source_target_pairs={{0,16},{4,20},{8,24},{12,28},{16,0},{20,4},{24,8},{28,12},{1,17},{... | collective-permute-start | bytes 18440 | tf_op jit(solution)/shard_map/ppermute | solution.py:356
  34.3 1.1 %collective-permute-start.13 = (bf16[2,3,512]{2,1,0:T(4,128)(2,1)S(1)}, bf16[2,3,512]{2,1,0:T(4,128)(2,1)S(1)}, u32[]{:S(2)}, u32[]{:S(2)}) collective-permute-start(bf16[2,3,512]{2,1,0:T(4,128)(2,1)S(1)} %get-tuple-element.45.tick_ref), channel_id=1, source_target_pairs={{0,8},{4,12},{8,0},{12,4},{16,24},{20,28},{24,16},{28,20},{1,9},{5... | collective-permute-start | bytes 18440 | tf_op jit(solution)/shard_map/ppermute | solution.py:356
  35.4 1.1 %shard_map.214 = (f32[8,128,128]{2,1,0:T(8,128)}, f32[8,128]{1,0:T(8,128)}, f32[1,8]{1,0:T(1,128)}) custom-call(bf16[2,3,512]{2,1,0:T(4,128)(2,1)S(1)} %get-tuple-element.45.tick_ref, f32[8,128,128]{2,1,0:T(8,128)S(1)} %bitcast.12, f32[8,128]{1,0:T(8,128)S(1)} %get-tuple-element.46.keys_ref, f32[8,128]{1,0:T(8,128)S(1)} %get-tuple-element.47.values_ref, ...), custom_call_target="tpu_custom_call" | custom-call | flops 20000000 | tf_op jit(solution)/shard_map/pallas_call | solution.py:22
  36.5 3.0 %collective-permute-done.12.refs_2_ = bf16[2,3,512]{2,1,0:T(4,128)(2,1)S(1)} collective-permute-done((bf16[2,3,512]{2,1,0:T(4,128)(2,1)S(1)}, bf16[2,3,512]{2,1,0:T(4,128)(2,1)S(1)}, u32[]{:S(2)}, u32[]{:S(2)}) %collective-permute-start.12) | collective-permute-done | bytes 6176 | tf_op jit(solution)/shard_map/ppermute | solution.py:356
  39.7 0.8 %shard_map.213 = bf16[8,512]{1,0:T(8,128)(2,1)} custom-call(f32[8,512]{1,0:T(8,128)S(1)} %shard_map.212.before_ref, f32[24,8]{1,0:T(8,128)S(1)} %get-tuple-element.34.mixing_ref, bf16[2,3,512]{2,1,0:T(4,128)(2,1)S(1)} %collective-permute-done.13.part_ref), custom_call_target="tpu_custom_call" | custom-call | flops 1000 | tf_op jit(solution)/shard_map/pallas_call | solution.py:22
  (20 shorter events, 1.4 us)
Async XLA Ops:
  3.0 5.4 %collective-permute-start.2 = (bf16[8,2048]{1,0:T(8,128)(2,1)S(1)}, bf16[8,2048]{1,0:T(8,128)(2,1)S(1)}, u32[]{:S(2)}, u32[]{:S(2)}) collective-permute-start(bf16[8,2048]{1,0:T(8,128)(2,1)S(1)} %get-tuple-element.29.tick_ref.refs_0_), channel_id=1, source_target_pairs={{0,3},{1,2},{2,1},{3,0},{4,7},{5,6},{6,5},{7,4},{8,11},{9,10},{10,... | collective-permute-start | bytes 98312 | tf_op jit(solution)/shard_map/ppermute | solution.py:356
  5.5 4.0 %collective-permute-start.1 = (bf16[8,2048]{1,0:T(8,128)(2,1)S(1)}, bf16[8,2048]{1,0:T(8,128)(2,1)S(1)}, u32[]{:S(2)}, u32[]{:S(2)}) collective-permute-start(bf16[8,2048]{1,0:T(8,128)(2,1)S(1)} %get-tuple-element.29.tick_ref.refs_0_), channel_id=1, source_target_pairs={{0,2},{1,3},{2,0},{3,1},{4,6},{5,7},{6,4},{7,5},{8,10},{9,11},{10,... | collective-permute-start | bytes 98312 | tf_op jit(solution)/shard_map/ppermute | solution.py:356
  6.2 3.3 %collective-permute-start = (bf16[8,2048]{1,0:T(8,128)(2,1)S(1)}, bf16[8,2048]{1,0:T(8,128)(2,1)S(1)}, u32[]{:S(2)}, u32[]{:S(2)}) collective-permute-start(bf16[8,2048]{1,0:T(8,128)(2,1)S(1)} %get-tuple-element.29.tick_ref.refs_0_), channel_id=1, source_target_pairs={{0,1},{1,0},{2,3},{3,2},{4,5},{5,4},{6,7},{7,6},{8,9},{9,8},{10,11... | collective-permute-start | bytes 98312 | tf_op jit(solution)/shard_map/ppermute | solution.py:356
  9.8 4.2 %collective-permute-start.3 = (bf16[4,6144]{1,0:T(4,128)(2,1)S(1)}, bf16[4,6144]{1,0:T(4,128)(2,1)S(1)}, u32[]{:S(2)}, u32[]{:S(2)}) collective-permute-start(bf16[4,6144]{1,0:T(4,128)(2,1)S(1)} %get-tuple-element.35.tick_ref), channel_id=1, source_target_pairs={{0,4},{4,0},{8,12},{12,8},{16,20},{20,16},{24,28},{28,24},{1,5},{5... | collective-permute-start | bytes 147464 | tf_op jit(solution)/shard_map/ppermute | solution.py:356
  14.1 4.2 %collective-permute-start.4 = (bf16[2,6144]{1,0:T(2,128)(2,1)S(1)}, bf16[2,6144]{1,0:T(2,128)(2,1)S(1)}, u32[]{:S(2)}, u32[]{:S(2)}) collective-permute-start(bf16[2,6144]{1,0:T(2,128)(2,1)S(1)} %get-tuple-element.38), channel_id=1, source_target_pairs={{0,8},{1,25},{2,10},{3,27},{4,12},{5,29},{6,14},{7,31},{8,0},{9,17... | collective-permute-start | bytes 73736 | tf_op jit(solution)/shard_map/ppermute | solution.py:366
  15.7 5.1 %collective-permute-start.5 = (bf16[2,6144]{1,0:T(2,128)(2,1)S(1)}, bf16[2,6144]{1,0:T(2,128)(2,1)S(1)}, u32[]{:S(2)}, u32[]{:S(2)}) collective-permute-start(bf16[2,6144]{1,0:T(2,128)(2,1)S(1)} %get-tuple-element.39), channel_id=1, source_target_pairs={{0,16},{1,17},{2,18},{3,19},{4,20},{5,21},{6,22},{7,23},{8,24},{9,... | collective-permute-start | bytes 73736 | tf_op jit(solution)/shard_map/ppermute | solution.py:366
  18.3 2.5 %collective-permute-start.6 = (bf16[2,6144]{1,0:T(2,128)(2,1)S(1)}, bf16[2,6144]{1,0:T(2,128)(2,1)S(1)}, u32[]{:S(2)}, u32[]{:S(2)}) collective-permute-start(bf16[2,6144]{1,0:T(2,128)(2,1)S(1)} %collective-permute-done.4.refs_1_), channel_id=1, source_target_pairs={{0,1},{1,0},{2,3},{3,2},{4,5},{5,4},{6,7},{7,6},{8,9},{9,8},{10,11... | collective-permute-start | bytes 73736 | tf_op jit(solution)/shard_map/ppermute | solution.py:356
  22.4 4.7 %collective-permute-start.8 = (bf16[24,1024]{1,0:T(8,128)(2,1)S(1)}, bf16[24,1024]{1,0:T(8,128)(2,1)S(1)}, u32[]{:S(2)}, u32[]{:S(2)}) collective-permute-start(bf16[24,1024]{1,0:T(8,128)(2,1)S(1)} %shard_map.206.tick_ref.own_ref), channel_id=1, source_target_pairs={{0,1},{1,0},{2,3},{3,2},{4,5},{5,4},{6,7},{7,6},{8,9},{9,8},{10,11... | collective-permute-start | bytes 147464 | tf_op jit(solution)/shard_map/ppermute | solution.py:356
  22.6 4.6 %collective-permute-start.7 = (bf16[24,1024]{1,0:T(8,128)(2,1)S(1)}, bf16[24,1024]{1,0:T(8,128)(2,1)S(1)}, u32[]{:S(2)}, u32[]{:S(2)}) collective-permute-start(bf16[24,1024]{1,0:T(8,128)(2,1)S(1)} %shard_map.206.tick_ref.own_ref), channel_id=1, source_target_pairs={{0,3},{1,2},{2,1},{3,0},{4,7},{5,6},{6,5},{7,4},{8,11},{9,10},{10,... | collective-permute-start | bytes 147464 | tf_op jit(solution)/shard_map/ppermute | solution.py:356
  23.4 4.2 %collective-permute-start.9 = (bf16[24,1024]{1,0:T(8,128)(2,1)S(1)}, bf16[24,1024]{1,0:T(8,128)(2,1)S(1)}, u32[]{:S(2)}, u32[]{:S(2)}) collective-permute-start(bf16[24,1024]{1,0:T(8,128)(2,1)S(1)} %shard_map.206.tick_ref.own_ref), channel_id=1, source_target_pairs={{0,2},{1,3},{2,0},{3,1},{4,6},{5,7},{6,4},{7,5},{8,10},{9,11},{10,... | collective-permute-start | bytes 147464 | tf_op jit(solution)/shard_map/ppermute | solution.py:356
  27.1 8.3 %copy-start = (f32[8,1,16384]{2,1,0:T(1,128)S(1)}, f32[8,1,16384]{2,1,0:T(1,128)}, u32[]{:S(2)}) copy-start(f32[8,1,16384]{2,1,0:T(1,128)} %param.27) | copy-start | bytes 1572868
  28.0 3.8 %collective-permute-start.10 = (bf16[4,3,512]{2,1,0:T(4,128)(2,1)S(1)}, bf16[4,3,512]{2,1,0:T(4,128)(2,1)S(1)}, u32[]{:S(2)}, u32[]{:S(2)}) collective-permute-start(bf16[4,3,512]{2,1,0:T(4,128)(2,1)S(1)} %get-tuple-element.41), channel_id=1, source_target_pairs={{0,4},{4,0},{8,12},{12,8},{16,20},{20,16},{24,28},{28,24},{1,5},{5... | collective-permute-start | bytes 36872 | tf_op jit(solution)/shard_map/ppermute | solution.py:356
  31.8 4.7 %collective-permute-start.11 = (bf16[2,3,512]{2,1,0:T(4,128)(2,1)S(1)}, bf16[2,3,512]{2,1,0:T(4,128)(2,1)S(1)}, u32[]{:S(2)}, u32[]{:S(2)}) collective-permute-start(bf16[2,3,512]{2,1,0:T(4,128)(2,1)S(1)} %get-tuple-element.43), channel_id=1, source_target_pairs={{0,16},{4,20},{8,24},{12,28},{16,0},{20,4},{24,8},{28,12},{1,17},{... | collective-permute-start | bytes 18440 | tf_op jit(solution)/shard_map/ppermute | solution.py:356
  34.1 5.4 %collective-permute-start.12 = (bf16[2,3,512]{2,1,0:T(4,128)(2,1)S(1)}, bf16[2,3,512]{2,1,0:T(4,128)(2,1)S(1)}, u32[]{:S(2)}, u32[]{:S(2)}) collective-permute-start(bf16[2,3,512]{2,1,0:T(4,128)(2,1)S(1)} %get-tuple-element.44), channel_id=1, source_target_pairs={{0,24},{4,28},{8,16},{12,20},{16,8},{20,12},{24,0},{28,4},{1,25},{... | collective-permute-start | bytes 18440 | tf_op jit(solution)/shard_map/ppermute | solution.py:356
  34.3 5.4 %collective-permute-start.13 = (bf16[2,3,512]{2,1,0:T(4,128)(2,1)S(1)}, bf16[2,3,512]{2,1,0:T(4,128)(2,1)S(1)}, u32[]{:S(2)}, u32[]{:S(2)}) collective-permute-start(bf16[2,3,512]{2,1,0:T(4,128)(2,1)S(1)} %get-tuple-element.45.tick_ref), channel_id=1, source_target_pairs={{0,8},{4,12},{8,0},{12,4},{16,24},{20,28},{24,16},{28,20},{1,9},{5... | collective-permute-start | bytes 18440 | tf_op jit(solution)/shard_map/ppermute | solution.py:356
